TPU v7x, 512 devices: a whole 4x4x16 slice. The times are simulated.
512 devices in a mesh: fs: 16 (over y, x), tp: 32 (over z, core).
Axes of the slice: x: 4, y: 4, z: 16, core: 2. Of those that a mesh axis runs over, the one named last changes fastest.
Arguments:
- x_later: bfloat16 [6144, 2048], P('fs'), may hold values from -6 to 6
- x_earlier: bfloat16 [6144, 2048], P('fs'), may hold values from -6 to 6
- cot_hidden: bfloat16 [6144, 4096], P('fs', 'tp'), may hold values from -6 to 6
- w_gate: bfloat16 [2048, 4096], P('fs', 'tp'), may hold values from -0.125 to 0.125
- w_up: bfloat16 [2048, 4096], P('fs', 'tp'), may hold values from -0.125 to 0.125
- grad_gate: float32 [2048, 4096], P('fs', 'tp'), may hold values from -192 to 192
- grad_up: float32 [2048, 4096], P('fs', 'tp'), may hold values from -192 to 192
Outputs:
- hidden_later: bfloat16 [6144, 4096], P('fs', 'tp')
- grad_input: bfloat16 [6144, 2048], P('fs')
- new_grad_gate: float32 [2048, 4096], P('fs', 'tp')
- new_grad_up: float32 [2048, 4096], P('fs', 'tp')
All inputs are finite; a program needn't handle non-finite values.
Results may differ from a plain program's by a relative error of at most 0.018.
Values may be sent and summed in bfloat16 or wider, within the bound.
A program may use at most 64 MiB of HBM per device.

v0:
```python
import jax
import jax.numpy as jnp
from jax import lax
from jax.sharding import PartitionSpec as P


def contract_last(left, right):
    return lax.dot_general(
        left, right, (((1,), (1,)), ((), ())), preferred_element_type=jnp.float32
    )


def contract_first(left, right):
    return lax.dot_general(
        left, right, (((0,), (0,)), ((), ())), preferred_element_type=jnp.float32
    )


def per_device(x_later, x_earlier, cot_hidden, w_gate, w_up, grad_gate, grad_up):
    hidden_width = w_gate.shape[1]
    whole_gate, whole_up = (
        lax.all_gather(w_gate, "fs", axis=0, tiled=True),
        lax.all_gather(w_up, "fs", axis=0, tiled=True),
    )
    gate_later = jnp.dot(x_later, whole_gate, preferred_element_type=jnp.float32)
    up_later = jnp.dot(x_later, whole_up, preferred_element_type=jnp.float32)
    gate_earlier = jnp.dot(x_earlier, whole_gate, preferred_element_type=jnp.float32)
    up_earlier = jnp.dot(x_earlier, whole_up, preferred_element_type=jnp.float32)
    hidden_later = (jax.nn.silu(gate_later) * up_later).astype(jnp.bfloat16)
    sigma = jax.nn.sigmoid(gate_earlier)
    cotangent = cot_hidden.astype(jnp.float32)
    delta_up = (cotangent * gate_earlier * sigma).astype(jnp.bfloat16)
    delta_gate = (cotangent * up_earlier * sigma * (1.0 + gate_earlier * (1.0 - sigma))).astype(
        jnp.bfloat16
    )
    grad_share = lax.psum_scatter(
        (contract_last(delta_gate, whole_gate) + contract_last(delta_up, whole_up)).astype(
            jnp.bfloat16
        ),
        "tp",
        scatter_dimension=0,
        tiled=True,
    )
    grad_input = lax.all_gather(grad_share, "tp", axis=0, tiled=True)
    deltas = jnp.concatenate([delta_gate, delta_up], 1)
    summed = lax.psum_scatter(
        contract_first(x_earlier, deltas).astype(jnp.bfloat16),
        "fs",
        scatter_dimension=0,
        tiled=True,
    ).astype(jnp.float32)
    new_grad_gate = grad_gate + summed[:, :hidden_width]
    new_grad_up = grad_up + summed[:, hidden_width:]
    return (hidden_later, grad_input, new_grad_gate, new_grad_up)


def solution(mesh):
    placed = (
        P("fs", None),
        P("fs", None),
        P("fs", "tp"),
        P("fs", "tp"),
        P("fs", "tp"),
        P("fs", "tp"),
        P("fs", "tp"),
    )
    return jax.shard_map(
        per_device,
        mesh=mesh,
        in_specs=placed,
        out_specs=(P("fs", "tp"), P("fs", None), P("fs", "tp"), P("fs", "tp")),
        check_vma=False,
    )
```

profile of v0, /device:TPU:1, one launch (start us, length us, event | category | flops | bytes accessed | tf_op | source)
XLA Modules:
  0.0 242.5 jit_solution(5092972627354294884)
XLA Ops:
  8.0 0.0 copy-start
  8.0 0.0 reduce-scatter.6.cloned.1.call-start
  8.1 20.1 %all_gather.10 = bf16[2048,128]{1,0:T(8,128)(2,1)S(1)} all-gather(bf16[128,128]{1,0:T(8,128)(2,1)} %param.11), channel_id=1, replica_groups=mesh['fs'=16,'tp'=32] {'fs'}, dimensions={0}, use_global_device_ids=true | all-gather | bytes 557056 | tf_op jit(solution)/shard_map/all_gather | solution.py:23
  28.1 17.9 %all_gather.9 = bf16[2048,128]{1,0:T(8,128)(2,1)S(1)} all-gather(bf16[128,128]{1,0:T(8,128)(2,1)} %param.10), channel_id=1, replica_groups=mesh['fs'=16,'tp'=32] {'fs'}, dimensions={0}, use_global_device_ids=true | all-gather | bytes 557056 | tf_op jit(solution)/shard_map/all_gather | solution.py:22
  46.1 0.0 copy-start.9
  46.1 1.7 fusion.7
  47.8 0.6 fusion.5
  48.4 0.7 fusion.1
  49.1 1.3 copy.37
  50.4 0.0 reduce-scatter.6.cloned.1.call-update
  50.4 0.0 all-gather.3.cloned.1.call-start
  50.5 0.6 fusion.13
  51.1 0.5 copy-done.4
  51.5 0.6 add_convert_fusion
  52.1 0.0 copy-start.7
  52.1 0.0 copy-start.8
  52.2 74.8 %fusion = bf16[16,2048]{1,0:T(8,128)(2,1)S(1)} fusion(bf16[384,2048]{1,0:T(8,128)(2,1)S(1)} %add_convert_fusion), kind=kCustom, calls=%all-reduce-scatter | all-reduce-scatter fusion | flops 1048577 | bytes 1640448
  127.0 3.4 %collective-permute-start.6 = (bf16[16,2048]{1,0:T(8,128)(2,1)S(1)}, bf16[16,2048]{1,0:T(8,128)(2,1)S(1)}, u32[]{:S(2)}, u32[]{:S(2)}) collective-permute-start(bf16[16,2048]{1,0:T(8,128)(2,1)S(1)} %fusion), channel_id=1, source_target_pairs={{0,7},{1,8},{2,9},{3,10},{4,11},{5,12},{6,13},{7,14},{8,15},{9,16}... | collective-permute-start | bytes 196616
  130.4 4.5 %collective-permute-start.5 = (bf16[16,2048]{1,0:T(8,128)(2,1)S(1)}, bf16[16,2048]{1,0:T(8,128)(2,1)S(1)}, u32[]{:S(2)}, u32[]{:S(2)}) collective-permute-start(bf16[16,2048]{1,0:T(8,128)(2,1)S(1)} %fusion), channel_id=1, source_target_pairs={{0,6},{1,7},{2,8},{3,9},{4,10},{5,11},{6,12},{7,13},{8,14},{9,15},... | collective-permute-start | bytes 196616
  134.9 6.2 %collective-permute-start.7 = (bf16[12,2048]{1,0:T(8,128)(2,1)S(1)}, bf16[12,2048]{1,0:T(8,128)(2,1)S(1)}, u32[]{:S(2)}, u32[]{:S(2)}) collective-permute-start(bf16[12,2048]{1,0:T(8,128)(2,1)S(1)} %slice.10), channel_id=1, source_target_pairs={{0,8},{1,9},{2,10},{3,11},{4,12},{5,13},{6,14},{7,15},{8,16},{9,17... | collective-permute-start | bytes 147464
  141.1 1.7 collective-permute-start.4
  142.8 6.4 %collective-permute-start.3 = (bf16[16,2048]{1,0:T(8,128)(2,1)S(1)}, bf16[16,2048]{1,0:T(8,128)(2,1)S(1)}, u32[]{:S(2)}, u32[]{:S(2)}) collective-permute-start(bf16[16,2048]{1,0:T(8,128)(2,1)S(1)} %fusion), channel_id=1, source_target_pairs={{0,4},{1,5},{2,6},{3,7},{4,8},{5,9},{6,10},{7,11},{8,12},{9,13},{1... | collective-permute-start | bytes 196616
  149.3 0.0 collective-permute-done.7
  149.3 1.6 collective-permute-start.2
  150.9 0.0 collective-permute-done.6
  150.9 2.8 %collective-permute-start.1 = (bf16[16,2048]{1,0:T(8,128)(2,1)S(1)}, bf16[16,2048]{1,0:T(8,128)(2,1)S(1)}, u32[]{:S(2)}, u32[]{:S(2)}) collective-permute-start(bf16[16,2048]{1,0:T(8,128)(2,1)S(1)} %fusion), channel_id=1, source_target_pairs={{0,2},{1,3},{2,4},{3,5},{4,6},{5,7},{6,8},{7,9},{8,10},{9,11},{10,... | collective-permute-start | bytes 196616
  153.7 0.0 collective-permute-done.5
  153.7 2.2 collective-permute-start
  155.9 1.3 dynamic-slice.4
  157.8 0.0 collective-permute-done.4
  157.8 0.0 collective-permute-done.3
  157.9 0.0 collective-permute-done.2
  157.9 0.0 collective-permute-done.1
  157.9 0.0 collective-permute-done
  157.9 1.5 concatenate.4
  159.4 0.7 dynamic-slice_bitcast_fusion
  160.0 0.0 all-gather.3.cloned.1.call-update
  160.1 0.1 copy.32
  160.2 0.0 copy-done.8
  160.2 0.1 copy.31
  160.3 0.0 copy-start.6
  160.3 2.1 fusion.12
  162.4 1.2 fusion.4
  163.6 0.9 copy.38
  164.6 0.7 copy.33
  165.4 0.7 copy.34
  166.1 65.4 %all-gather.3.cloned.1.call-done = bf16[32,12,2048]{2,1,0:T(8,128)(2,1)} async-done(((bf16[1,12,2048]{2,1,0:T(8,128)(2,1)}), bf16[32,12,2048]{2,1,0:T(8,128)(2,1)}) %all-gather.3.cloned.1.call-update) | async-done | bytes 1572880 | tf_op jit(solution)/shard_map/all_gather | solution.py:44
  231.4 3.6 %reshape.9 = bf16[384,2048]{1,0:T(8,128)(2,1)} reshape(bf16[32,12,2048]{2,1,0:T(8,128)(2,1)} %all-gather.3.cloned.1.call-done) | data formatting | bytes 3145728
  (17 shorter events, 0.1 us)
Async XLA Ops:
  8.0 38.1 %copy-start = (bf16[384,2048]{1,0:T(8,128)(2,1)S(1)}, bf16[384,2048]{1,0:T(8,128)(2,1)}, u32[]{:S(2)}) copy-start(bf16[384,2048]{1,0:T(8,128)(2,1)} %param.8) | copy-start | bytes 4718596
  8.0 155.6 %reduce-scatter.6.cloned.1.call-start = ((), (), s32[]{:S(2)}) async-start(), calls=%async_computation.2 | async-start | bytes 1114112
  28.1 19.6 %copy-start.3 = (bf16[2048,128]{1,0:T(8,128)(2,1)}, bf16[2048,128]{1,0:T(8,128)(2,1)S(1)}, u32[]{:S(2)}) copy-start(bf16[2048,128]{1,0:T(8,128)(2,1)S(1)} %all_gather.10) | copy-start | bytes 1572868
  46.1 4.4 %copy-start.1 = (bf16[2048,128]{1,0:T(8,128)(2,1)}, bf16[2048,128]{1,0:T(8,128)(2,1)S(1)}, u32[]{:S(2)}) copy-start(bf16[2048,128]{1,0:T(8,128)(2,1)S(1)} %all_gather.9) | copy-start | bytes 1572868
  46.1 1.7 copy-start.9
  50.4 181.0 %all-gather.3.cloned.1.call-start = ((), (), s32[]{:S(2)}) async-start(), calls=%async_computation.1 | async-start | bytes 2162688 | tf_op jit(solution)/shard_map/all_gather | solution.py:44
  50.5 1.0 copy-start.4
  52.1 107.9 %copy-start.7 = (f32[128,128]{1,0:T(8,128)S(1)}, f32[128,128]{1,0:T(8,128)}, u32[]{:S(2)}) copy-start(f32[128,128]{1,0:T(8,128)} %param.13) | copy-start | bytes 196612
  52.1 108.0 %copy-start.8 = (f32[128,128]{1,0:T(8,128)S(1)}, f32[128,128]{1,0:T(8,128)}, u32[]{:S(2)}) copy-start(f32[128,128]{1,0:T(8,128)} %param.12) | copy-start | bytes 196612
  127.0 33.3 %copy-start.2 = (bf16[2048,128]{1,0:T(8,128)(2,1)S(1)}, bf16[2048,128]{1,0:T(8,128)(2,1)}, u32[]{:S(2)}) copy-start(bf16[2048,128]{1,0:T(8,128)(2,1)} %copy-done.1) | copy-start | bytes 1572868
  127.0 24.0 %collective-permute-start.6 = (bf16[16,2048]{1,0:T(8,128)(2,1)S(1)}, bf16[16,2048]{1,0:T(8,128)(2,1)S(1)}, u32[]{:S(2)}, u32[]{:S(2)}) collective-permute-start(bf16[16,2048]{1,0:T(8,128)(2,1)S(1)} %fusion), channel_id=1, source_target_pairs={{0,7},{1,8},{2,9},{3,10},{4,11},{5,12},{6,13},{7,14},{8,15},{9,16}... | collective-permute-start | bytes 196616
  130.4 23.3 %collective-permute-start.5 = (bf16[16,2048]{1,0:T(8,128)(2,1)S(1)}, bf16[16,2048]{1,0:T(8,128)(2,1)S(1)}, u32[]{:S(2)}, u32[]{:S(2)}) collective-permute-start(bf16[16,2048]{1,0:T(8,128)(2,1)S(1)} %fusion), channel_id=1, source_target_pairs={{0,6},{1,7},{2,8},{3,9},{4,10},{5,11},{6,12},{7,13},{8,14},{9,15},... | collective-permute-start | bytes 196616
  134.9 14.4 %collective-permute-start.7 = (bf16[12,2048]{1,0:T(8,128)(2,1)S(1)}, bf16[12,2048]{1,0:T(8,128)(2,1)S(1)}, u32[]{:S(2)}, u32[]{:S(2)}) collective-permute-start(bf16[12,2048]{1,0:T(8,128)(2,1)S(1)} %slice.10), channel_id=1, source_target_pairs={{0,8},{1,9},{2,10},{3,11},{4,12},{5,13},{6,14},{7,15},{8,16},{9,17... | collective-permute-start | bytes 147464
  141.1 16.7 %collective-permute-start.4 = (bf16[16,2048]{1,0:T(8,128)(2,1)S(1)}, bf16[16,2048]{1,0:T(8,128)(2,1)S(1)}, u32[]{:S(2)}, u32[]{:S(2)}) collective-permute-start(bf16[16,2048]{1,0:T(8,128)(2,1)S(1)} %fusion), channel_id=1, source_target_pairs={{0,5},{1,6},{2,7},{3,8},{4,9},{5,10},{6,11},{7,12},{8,13},{9,14},{... | collective-permute-start | bytes 196616
  142.8 15.0 %collective-permute-start.3 = (bf16[16,2048]{1,0:T(8,128)(2,1)S(1)}, bf16[16,2048]{1,0:T(8,128)(2,1)S(1)}, u32[]{:S(2)}, u32[]{:S(2)}) collective-permute-start(bf16[16,2048]{1,0:T(8,128)(2,1)S(1)} %fusion), channel_id=1, source_target_pairs={{0,4},{1,5},{2,6},{3,7},{4,8},{5,9},{6,10},{7,11},{8,12},{9,13},{1... | collective-permute-start | bytes 196616
  149.3 8.6 %collective-permute-start.2 = (bf16[16,2048]{1,0:T(8,128)(2,1)S(1)}, bf16[16,2048]{1,0:T(8,128)(2,1)S(1)}, u32[]{:S(2)}, u32[]{:S(2)}) collective-permute-start(bf16[16,2048]{1,0:T(8,128)(2,1)S(1)} %fusion), channel_id=1, source_target_pairs={{0,3},{1,4},{2,5},{3,6},{4,7},{5,8},{6,9},{7,10},{8,11},{9,12},{10... | collective-permute-start | bytes 196616
  150.9 6.9 %collective-permute-start.1 = (bf16[16,2048]{1,0:T(8,128)(2,1)S(1)}, bf16[16,2048]{1,0:T(8,128)(2,1)S(1)}, u32[]{:S(2)}, u32[]{:S(2)}) collective-permute-start(bf16[16,2048]{1,0:T(8,128)(2,1)S(1)} %fusion), channel_id=1, source_target_pairs={{0,2},{1,3},{2,4},{3,5},{4,6},{5,7},{6,8},{7,9},{8,10},{9,11},{10,... | collective-permute-start | bytes 196616
  153.7 4.2 %collective-permute-start = (bf16[16,2048]{1,0:T(8,128)(2,1)S(1)}, bf16[16,2048]{1,0:T(8,128)(2,1)S(1)}, u32[]{:S(2)}, u32[]{:S(2)}) collective-permute-start(bf16[16,2048]{1,0:T(8,128)(2,1)S(1)} %fusion), channel_id=1, source_target_pairs={{0,1},{1,2},{2,3},{3,4},{4,5},{5,6},{6,7},{7,8},{8,9},{9,10},{10,1... | collective-permute-start | bytes 196616
  159.4 3.0 %copy-start.5 = (bf16[2048,128]{1,0:T(8,128)(2,1)S(1)}, bf16[2048,128]{1,0:T(8,128)(2,1)}, u32[]{:S(2)}) copy-start(bf16[2048,128]{1,0:T(8,128)(2,1)} %copy-done.3) | copy-start | bytes 1572868
  160.3 2.1 copy-start.6
Sparse Core Ops, SparseCore 0:
  50.6 100.0 reduce-scatter.5
Sparse Core Ops, SparseCore 1:
  160.1 71.2 all-gather.2
where the time goes:
time: 243 us; the launch traced here: 242 us
  blocking collectives  113 us (47%)
  waiting for transfers between devices  65.4 us (27%)
  starting transfers between devices  28.9 us (12%)
  between operations  16.5 us (7%)
  local copies, waits for them, and re-layouts  11.4 us (5%)
  matrix products  7.43 us (3%)
    unnamed x1, blocking collectives  74.8 us
    all_gather x1, waiting for transfers between devices, per_device(): grad_input = lax.all_gather(grad_share, 'tp', axis=0, tiled=True)  65.4 us
    unnamed x9, starting transfers between devices  28.9 us
    all_gather x1, blocking collectives, per_device(): lax.all_gather(w_up, 'fs', axis=0, tiled=True)  20.1 us
    all_gather x1, blocking collectives, per_device(): lax.all_gather(w_gate, 'fs', axis=0, tiled=True)  17.9 us
    unnamed x31, local copies, waits for them, and re-layouts  11.4 us
  transfers between devices with their start and end apart: 10, of which 1 were waited for; matrix products, arithmetic and copies ran while one was open for 35% of the time, Pallas kernels for 0%

commit v1 on v0

v1 whole, which is shorter than its diff:
```python
import functools

import jax
import jax.numpy as jnp
from jax import lax
from jax.experimental import pallas as pl
from jax.experimental.pallas import tpu as pltpu
from jax.sharding import PartitionSpec as P

MESH = pl.DeviceIdType.MESH
SUB = 2
F32 = jnp.float32
BF16 = jnp.bfloat16


def kernel(
    nz,
    xl_h, xe_h, cot_h, wg_h, wu_h, gg_h, gu_h, hid_o, gi_o, ngg_o, ngu_o,
    xl, xe, cot, gg, gu, hid, ngg, ngu,
    wq, wall,
    dcat, dwt, dwr, dw_own,
    pc, ps, pown, sp, sm, rp, rm, gi,
    in_sem, out_sem, gi_out_sem,
    ag_send, ag_recv, dw_send, dw_recv, ps_send, ps_recv,
    rsp_send, rsp_recv, rsm_send, rsm_recv,
    agp_send, agp_recv, agm_send, agm_recv, d2_send, d2_recv,
):
    rows = xe.shape[0]
    blocks = xe.shape[1] // 128
    up = nz // 2
    dn = nz - 1 - up
    per = blocks // nz
    crows = per * rows
    piece = crows // SUB

    f = lax.axis_index("fs")
    t = lax.axis_index("tp")
    y, x = f // 4, f % 4
    z, core = t // 2, t % 2

    loads = [
        pltpu.make_async_copy(wg_h, wq.at[:, 0, :, pl.ds(0, 128)], in_sem.at[0]),
        pltpu.make_async_copy(wu_h, wq.at[:, 0, :, pl.ds(128, 128)], in_sem.at[1]),
        pltpu.make_async_copy(xe_h, xe, in_sem.at[2]),
        pltpu.make_async_copy(cot_h, cot, in_sem.at[3]),
        pltpu.make_async_copy(xl_h, xl, in_sem.at[4]),
        pltpu.make_async_copy(gg_h, gg, in_sem.at[5]),
        pltpu.make_async_copy(gu_h, gu, in_sem.at[6]),
    ]
    for load in loads:
        load.start()

    x1 = x + 1 - 2 * (x % 2)
    y1 = y + 1 - 2 * (y % 2)
    flips = [y * 4 + x1, y * 4 + (3 - x), y1 * 4 + x, (3 - y) * 4 + x]
    right = {"fs": f, "tp": ((z + 1) % nz) * 2 + core}
    left = {"fs": f, "tp": ((z + nz - 1) % nz) * 2 + core}
    partner = {"fs": f, "tp": z * 2 + 1 - core}

    barrier = pltpu.get_barrier_semaphore()
    for g in flips:
        pl.semaphore_signal(barrier, inc=1, device_id={"fs": g, "tp": t}, device_id_type=MESH)
    for who in (partner, right, left):
        pl.semaphore_signal(barrier, inc=1, device_id=who, device_id_type=MESH)
    pl.semaphore_wait(barrier, 7)

    def gather_send(q, s, first, count):
        pltpu.make_async_remote_copy(
            src_ref=wq.at[q, pl.ds(first, count)],
            dst_ref=wq.at[q, pl.ds(first + 2**s, count)],
            send_sem=ag_send,
            recv_sem=ag_recv.at[q, s],
            device_id={"fs": flips[(q + s) % 4], "tp": t},
            device_id_type=MESH,
        ).start()

    def gather_wait(q, s):
        got = wq.at[q, pl.ds(2**s, 2**s)]
        pltpu.make_async_copy(got, got, ag_recv.at[q, s]).wait()

    loads[0].wait()
    loads[1].wait()
    for s in range(4):
        for q in range(4):
            gather_send(q, s, 0, 1)
    for a in range(3):
        for q in range(4):
            gather_wait(q, a)
            for s in range(a + 1, 4):
                gather_send(q, s, 2**a, 2**a)
    for q in range(4):
        gather_wait(q, 3)

    for q in range(4):
        for i in range(16):
            bits = [(q + b) % 4 for b in range(4) if (i >> b) & 1]
            ox = x
            oy = y
            if 0 in bits:
                ox = ox + 1 - 2 * (ox % 2)
            if 1 in bits:
                ox = 3 - ox
            if 2 in bits:
                oy = oy + 1 - 2 * (oy % 2)
            if 3 in bits:
                oy = 3 - oy
            start = pl.multiple_of((oy * 4 + ox) * 128 + 32 * q, 32)
            wall[pl.ds(start, 32), :] = wq[q, i]

    loads[2].wait()
    loads[3].wait()
    both = jnp.dot(xe[...], wall[...], preferred_element_type=F32)
    gate, upv = both[:, :128], both[:, 128:]
    sigma = jax.nn.sigmoid(gate)
    cotangent = cot[...].astype(F32)
    delta_up = cotangent * gate * sigma
    delta_gate = cotangent * upv * sigma * (1.0 + gate * (1.0 - sigma))
    dcat[:, pl.ds(0, 128)] = delta_gate.astype(BF16)
    dcat[:, pl.ds(128, 128)] = delta_up.astype(BF16)

    def partial_block(d, b):
        first = pl.multiple_of((d * per + b) * 128, 128)
        return lax.dot_general(
            dcat[...], wall[pl.ds(first, 128), :], (((1,), (1,)), ((), ())),
            preferred_element_type=F32,
        )

    def weight_gradients():
        turned = jnp.transpose(dcat[...].astype(F32)).astype(BF16)
        for i in range(16):
            to = (f + i) % 16
            first = pl.multiple_of(to * 128, 128)
            block = jnp.dot(turned, xe[:, pl.ds(first, 128)], preferred_element_type=F32)
            if i == 0:
                dw_own[...] = block
            else:
                dwt[i - 1] = block.astype(BF16)
                pltpu.make_async_remote_copy(
                    src_ref=dwt.at[i - 1],
                    dst_ref=dwr.at[i - 1],
                    send_sem=dw_send,
                    recv_sem=dw_recv.at[i - 1],
                    device_id={"fs": to, "tp": t},
                    device_id_type=MESH,
                ).start()

    def weight_gradients_done():
        total = dw_own[...]
        for i in range(15):
            pltpu.make_async_copy(dwr.at[i], dwr.at[i], dw_recv.at[i]).wait()
            total = total + dwr[i].astype(F32)
        loads[5].wait()
        loads[6].wait()
        ngg[...] = gg[...] + jnp.transpose(total[:128])
        ngu[...] = gu[...] + jnp.transpose(total[128:])
        pltpu.make_async_copy(ngg, ngg_o, out_sem.at[0]).start()
        pltpu.make_async_copy(ngu, ngu_o, out_sem.at[1]).start()

    def later():
        loads[4].wait()
        both = jnp.dot(xl[...], wall[...], preferred_element_type=F32)
        gate, upv = both[:, :128], both[:, 128:]
        hid[...] = (gate * jax.nn.sigmoid(gate) * upv).astype(BF16)
        pltpu.make_async_copy(hid, hid_o, out_sem.at[2]).start()

    def put_out(o):
        for b in range(per):
            first = pl.multiple_of((o * per + b) * 128, 128)
            pltpu.make_async_copy(
                gi.at[o, pl.ds(b * rows, rows)], gi_o.at[:, pl.ds(first, 128)], gi_out_sem
            ).start()

    def at(k):
        return pl.ds(k * piece, piece)

    @pl.when(core == 0)
    def _():
        def give(d):
            for b in range(per):
                pown[d, pl.ds(b * rows, rows)] = partial_block(d, b).astype(BF16)
            pltpu.make_async_remote_copy(
                src_ref=pown.at[d], dst_ref=ps.at[d], send_sem=ps_send, recv_sem=ps_recv.at[d],
                device_id=partner, device_id_type=MESH,
            ).start()

        for s in range(up):
            give((z + up - s) % nz)
            if s < dn:
                give((z + nz - dn + s) % nz)
        give(z)
        weight_gradients()
        later()
        weight_gradients_done()
        order = [z]
        for s in range(1, up + 1):
            order.append((z + nz - s) % nz)
            if s <= dn:
                order.append((z + s) % nz)
        for o in order:
            for k in range(SUB):
                pltpu.make_async_copy(gi.at[o, at(k)], gi.at[o, at(k)], d2_recv.at[o, k]).wait()
            put_out(o)
        pltpu.make_async_copy(pown, pown, ps_send).wait()

    @pl.when(core == 1)
    def _():
        def take(d):
            for b in range(per):
                pc[d, pl.ds(b * rows, rows)] = partial_block(d, b)
            pltpu.make_async_copy(ps.at[d], ps.at[d], ps_recv.at[d]).wait()
            pc[d] = pc[d] + ps[d].astype(F32)

        def forward(src, dst, send_sem, recv_sem, who):
            pltpu.make_async_remote_copy(
                src_ref=src, dst_ref=dst, send_sem=send_sem, recv_sem=recv_sem,
                device_id=who, device_id_type=MESH,
            ).start()

        def arrived(ref, sem):
            pltpu.make_async_copy(ref, ref, sem).wait()

        take((z + up) % nz)
        if dn > 0:
            take((z + nz - dn) % nz)
        for s in range(up):
            for k in range(SUB):
                value = pc[(z + up - s) % nz, at(k)]
                if s > 0:
                    arrived(rp.at[s - 1, at(k)], rsp_recv.at[s - 1, k])
                    value = value + rp[s - 1, at(k)].astype(F32)
                sp[s, at(k)] = value.astype(BF16)
                forward(sp.at[s, at(k)], rp.at[s, at(k)], rsp_send, rsp_recv.at[s, k], right)
                if s < dn:
                    value = pc[(z + nz - dn + s) % nz, at(k)]
                    if s > 0:
                        arrived(rm.at[s - 1, at(k)], rsm_recv.at[s - 1, k])
                        value = value + rm[s - 1, at(k)].astype(F32)
                    sm[s, at(k)] = value.astype(BF16)
                    forward(sm.at[s, at(k)], rm.at[s, at(k)], rsm_send, rsm_recv.at[s, k], left)
            if s + 1 < up:
                take((z + up - s - 1) % nz)
            else:
                take(z)
            if s + 1 < dn:
                take((z + nz - dn + s + 1) % nz)
            if s == min(2, up - 1):
                weight_gradients()

        for k in range(SUB):
            value = pc[z, at(k)]
            arrived(rp.at[up - 1, at(k)], rsp_recv.at[up - 1, k])
            value = value + rp[up - 1, at(k)].astype(F32)
            if dn > 0:
                arrived(rm.at[dn - 1, at(k)], rsm_recv.at[dn - 1, k])
                value = value + rm[dn - 1, at(k)].astype(F32)
            gi[z, at(k)] = value.astype(BF16)
            mine = gi.at[z, at(k)]
            forward(mine, mine, agp_send, agp_recv.at[0, k], right)
            if dn > 0:
                forward(mine, mine, agm_send, agm_recv.at[0, k], left)
            forward(mine, mine, d2_send, d2_recv.at[z, k], partner)
        put_out(z)

        for s in range(1, up + 1):
            low = (z + nz - s) % nz
            high = (z + s) % nz
            for k in range(SUB):
                part = gi.at[low, at(k)]
                arrived(part, agp_recv.at[s - 1, k])
                if s < up:
                    forward(part, part, agp_send, agp_recv.at[s, k], right)
                forward(part, part, d2_send, d2_recv.at[low, k], partner)
                if s <= dn:
                    part = gi.at[high, at(k)]
                    arrived(part, agm_recv.at[s - 1, k])
                    if s < dn:
                        forward(part, part, agm_send, agm_recv.at[s, k], left)
                    forward(part, part, d2_send, d2_recv.at[high, k], partner)
            put_out(low)
            if s <= dn:
                put_out(high)
            if s == 1:
                later()
            if s == min(3, up):
                weight_gradients_done()

        arrived(sp, rsp_send)
        arrived(gi.at[pl.ds(0, up)], agp_send)
        if dn > 0:
            arrived(sm.at[pl.ds(0, dn)], rsm_send)
            arrived(gi.at[pl.ds(0, dn)], agm_send)
        arrived(gi, d2_send)

    pltpu.make_async_copy(wq.at[:, pl.ds(0, 15)], wq.at[:, pl.ds(0, 15)], ag_send).wait()
    pltpu.make_async_copy(dwt, dwt, dw_send).wait()
    pltpu.make_async_copy(gi, gi, gi_out_sem).wait()
    pltpu.make_async_copy(ngg, ngg_o, out_sem.at[0]).wait()
    pltpu.make_async_copy(ngu, ngu_o, out_sem.at[1]).wait()
    pltpu.make_async_copy(hid, hid_o, out_sem.at[2]).wait()


def per_device(nz, x_later, x_earlier, cot_hidden, w_gate, w_up, grad_gate, grad_up):
    rows, width = x_later.shape
    up = nz // 2
    dn = nz - 1 - up
    crows = (width // 128 // nz) * rows
    dma = pltpu.SemaphoreType.DMA
    any_spec = pl.BlockSpec(memory_space=pl.ANY)
    return pl.pallas_call(
        functools.partial(kernel, nz),
        out_shape=(
            jax.ShapeDtypeStruct((rows, 128), BF16),
            jax.ShapeDtypeStruct((rows, width), BF16),
            jax.ShapeDtypeStruct((128, 128), F32),
            jax.ShapeDtypeStruct((128, 128), F32),
        ),
        in_specs=[any_spec] * 7,
        out_specs=(any_spec,) * 4,
        scratch_shapes=[
            pltpu.VMEM((rows, width), BF16),
            pltpu.VMEM((rows, width), BF16),
            pltpu.VMEM((rows, 128), BF16),
            pltpu.VMEM((128, 128), F32),
            pltpu.VMEM((128, 128), F32),
            pltpu.VMEM((rows, 128), BF16),
            pltpu.VMEM((128, 128), F32),
            pltpu.VMEM((128, 128), F32),
            pltpu.VMEM((4, 16, 32, 256), BF16),
            pltpu.VMEM((width, 256), BF16),
            pltpu.VMEM((rows, 256), BF16),
            pltpu.VMEM((15, 256, 128), BF16),
            pltpu.VMEM((15, 256, 128), BF16),
            pltpu.VMEM((256, 128), F32),
            pltpu.VMEM((nz, crows, 128), F32),
            pltpu.VMEM((nz, crows, 128), BF16),
            pltpu.VMEM((nz, crows, 128), BF16),
            pltpu.VMEM((up, crows, 128), BF16),
            pltpu.VMEM((max(dn, 1), crows, 128), BF16),
            pltpu.VMEM((up, crows, 128), BF16),
            pltpu.VMEM((max(dn, 1), crows, 128), BF16),
            pltpu.VMEM((nz, crows, 128), BF16),
            dma((7,)),
            dma((3,)),
            dma,
            dma,
            dma((4, 4)),
            dma,
            dma((15,)),
            dma,
            dma((nz,)),
            dma,
            dma((up, SUB)),
            dma,
            dma((max(dn, 1), SUB)),
            dma,
            dma((up, SUB)),
            dma,
            dma((max(dn, 1), SUB)),
            dma,
            dma((nz, SUB)),
        ],
        compiler_params=pltpu.CompilerParams(
            collective_id=0, has_side_effects=True, vmem_limit_bytes=48 * 1024 * 1024
        ),
        name="step",
    )(
        x_later,
        x_earlier,
        cot_hidden,
        w_gate.reshape(4, 32, 128),
        w_up.reshape(4, 32, 128),
        grad_gate,
        grad_up,
    )


def solution(mesh):
    placed = (
        P("fs", None),
        P("fs", None),
        P("fs", "tp"),
        P("fs", "tp"),
        P("fs", "tp"),
        P("fs", "tp"),
        P("fs", "tp"),
    )
    return jax.shard_map(
        functools.partial(per_device, mesh.shape["tp"] // 2),
        mesh=mesh,
        in_specs=placed,
        out_specs=(P("fs", "tp"), P("fs", None), P("fs", "tp"), P("fs", "tp")),
        check_vma=False,
    )
```

time: 243 us -> 87.2 us (0.36)
  blocking collectives: 113 us -> 0 us
  Pallas kernels: 0 us -> 76.2 us
  waiting for transfers between devices: 65.4 us -> 0 us
  starting transfers between devices: 28.9 us -> 0 us
  between operations: 16.5 us -> 0.66 us
  matrix products: 7.43 us -> 0 us
    pallas_call x0 -> x1, Pallas kernels: none -> 76.2 us  [per_device(): pl.pallas_call(functools.partial(kernel, nz), out_shape=(jax.ShapeDtypeSt...]
    unnamed x1 -> x0, blocking collectives: 74.8 us -> none
    all_gather x1 -> x0, waiting for transfers between devices: 65.4 us -> none  [per_device(): grad_input = lax.all_gather(grad_share, 'tp', axis=0, tiled=True)]
    all_gather x2 -> x0, blocking collectives: 38 us -> none  [the longest x1 20.1 us: per_device(): lax.all_gather(w_up, 'fs', axis=0, tiled=True)]
    unnamed x9 -> x0, starting transfers between devices: 28.9 us -> none
    dot_general x7 -> x0, matrix products: 7.43 us -> none  [the longest x1 2.09 us: per_device(): jnp.dot(x_later, whole_gate, preferred_element_type=jnp.float32)]
    unnamed x31 -> x18, local copies, waits for them, and re-layouts: 11.4 us -> 9.94 us
  transfers between devices with their start and end apart: 10 -> 0, of which waited for: 1 -> 0; matrix products, arithmetic and copies ran while one was open for 35% -> 0% of each run, Pallas kernels for 0% -> 0%
where the time goes in v1:
time: 87.2 us; the launch traced here: 86.8 us
  Pallas kernels  76.2 us (87%)
  local copies, waits for them, and re-layouts  9.94 us (11%)
    pallas_call x1, Pallas kernels, per_device(): pl.pallas_call(functools.partial(kernel, nz), out_shape=(jax.ShapeDtypeSt...  76.2 us
    unnamed x18, local copies, waits for them, and re-layouts  9.94 us

profile of v1, /device:TPU:1, one launch (start us, length us, event | category | flops | bytes accessed | tf_op | source)
XLA Modules:
  0.0 86.8 jit_solution(10063758866095800321)
XLA Ops:
  0.6 0.0 copy-start
  0.6 1.4 %copy-done = bf16[384,2048]{1,0:T(8,128)(2,1)S(1)} copy-done((bf16[384,2048]{1,0:T(8,128)(2,1)S(1)}, bf16[384,2048]{1,0:T(8,128)(2,1)}, u32[]{:S(2)}) %copy-start) | copy-done | bytes 1572888
  2.0 0.0 copy-start.1
  2.0 1.4 %copy-done.1 = bf16[384,2048]{1,0:T(8,128)(2,1)S(1)} copy-done((bf16[384,2048]{1,0:T(8,128)(2,1)S(1)}, bf16[384,2048]{1,0:T(8,128)(2,1)}, u32[]{:S(2)}) %copy-start.1) | copy-done | bytes 1572888
  3.5 0.0 copy-start.2
  3.5 0.9 %copy-done.2 = bf16[384,128]{1,0:T(8,128)(2,1)S(1)} copy-done((bf16[384,128]{1,0:T(8,128)(2,1)S(1)}, bf16[384,128]{1,0:T(8,128)(2,1)}, u32[]{:S(2)}) %copy-start.2) | copy-done | bytes 98328
  4.3 0.0 copy-start.3
  4.3 0.8 copy-done.3
  5.2 0.0 copy-start.4
  5.2 0.8 copy-done.4
  6.0 0.0 copy-start.5
  6.0 0.8 copy-done.5
  6.8 0.0 copy-start.6
  6.8 0.8 copy-done.6
  7.5 76.2 %step.1 = (bf16[384,128]{1,0:T(8,128)(2,1)S(1)}, bf16[384,2048]{1,0:T(8,128)(2,1)S(1)}, f32[128,128]{1,0:T(8,128)S(1)}, f32[128,128]{1,0:T(8,128)S(1)}) custom-call(bf16[384,2048]{1,0:T(8,128)(2,1)S(1)} %copy-done, bf16[384,2048]{1,0:T(8,128)(2,1)S(1)} %copy-done.1, bf16[384,128]{1,0:T(8,128)(2,1)S(1)} %copy-done.2, bf16[4,32,128]{2,1,0:T(8,128)(2,1)S(1)} %bitcast.2, ...), custom_call_target="tpu_custom_call" | custom-call | tf_op jit(solution)/shard_map/step/pallas_call | solution.py:309
  83.7 0.6 copy.15
  84.4 1.1 %copy.16 = bf16[384,2048]{1,0:T(8,128)(2,1)} copy(bf16[384,2048]{1,0:T(8,128)(2,1)S(1)} %get-tuple-element.9) | data formatting | bytes 3145728
  85.5 0.6 copy.17
  86.1 0.6 copy.18
Async XLA Ops:
  0.6 1.4 %copy-start = (bf16[384,2048]{1,0:T(8,128)(2,1)S(1)}, bf16[384,2048]{1,0:T(8,128)(2,1)}, u32[]{:S(2)}) copy-start(bf16[384,2048]{1,0:T(8,128)(2,1)} %xl_h.1) | copy-start | bytes 4718596
  2.0 1.4 %copy-start.1 = (bf16[384,2048]{1,0:T(8,128)(2,1)S(1)}, bf16[384,2048]{1,0:T(8,128)(2,1)}, u32[]{:S(2)}) copy-start(bf16[384,2048]{1,0:T(8,128)(2,1)} %xe_h.1) | copy-start | bytes 4718596
  3.5 0.9 %copy-start.2 = (bf16[384,128]{1,0:T(8,128)(2,1)S(1)}, bf16[384,128]{1,0:T(8,128)(2,1)}, u32[]{:S(2)}) copy-start(bf16[384,128]{1,0:T(8,128)(2,1)} %cot_h.1) | copy-start | bytes 294916
  4.3 0.8 copy-start.3
  5.2 0.8 copy-start.4
  6.0 0.8 copy-start.5
  6.8 0.8 copy-start.6

commit v2 on v0

v2 whole, which is shorter than its diff:
```python
import functools

import jax
import jax.numpy as jnp
from jax import lax
from jax.experimental import pallas as pl
from jax.experimental.pallas import tpu as pltpu
from jax.sharding import PartitionSpec as P

MESH = pl.DeviceIdType.MESH
SUB = 2
F32 = jnp.float32
BF16 = jnp.bfloat16


def copy_to(src, dst, send_sem, recv_sem, who):
    pltpu.make_async_remote_copy(
        src_ref=src, dst_ref=dst, send_sem=send_sem, recv_sem=recv_sem,
        device_id=who, device_id_type=MESH,
    ).start()


def arrived(ref, sem):
    pltpu.make_async_copy(ref, ref, sem).wait()


def kernel(
    nz,
    xl_h, xe_h, cot_h, wg_h, wu_h, gg_h, gu_h, hid, gi, ngg, ngu,
    xl, xe, cot, gg, gu,
    wq, wall,
    dcat, dwt, dwr, hid_other,
    pc, ring_s, ring_r,
    in_sem, give_send, give_recv, ag_send, ag_recv,
    share_send, share_recv, dw_send, dw_recv, hid_send, hid_recv,
    rs_send, rs_recv, gather_send_sem, gather_recv, d2_send, d2_recv,
):
    rows = xe.shape[0]
    piece = rows // SUB
    half = nz // 2
    steps = nz // 4

    f = lax.axis_index("fs")
    t = lax.axis_index("tp")
    y, x = f // 4, f % 4
    z, core = t // 2, t % 2
    x1 = x + 1 - 2 * (x % 2)
    y1 = y + 1 - 2 * (y % 2)
    flips = [y * 4 + x1, y * 4 + (3 - x), y1 * 4 + x, (3 - y) * 4 + x]
    partner = {"fs": f, "tp": z * 2 + 1 - core}

    def along(by):
        return {"fs": f, "tp": ((z + nz + by) % nz) * 2 + core}

    def at(k):
        return pl.ds(k * piece, piece)

    load_xe = pltpu.make_async_copy(xe_h, xe, in_sem.at[0])
    load_gg = pltpu.make_async_copy(gg_h, gg, in_sem.at[1])
    load_gu = pltpu.make_async_copy(gu_h, gu, in_sem.at[2])
    barrier = pltpu.get_barrier_semaphore()

    def new_gradients(total):
        load_gg.wait()
        load_gu.wait()
        ngg[...] = gg[...] + jnp.transpose(total[:128])
        ngu[...] = gu[...] + jnp.transpose(total[128:])

    @pl.when(core == 0)
    def _():
        load_xl = pltpu.make_async_copy(xl_h, xl, in_sem.at[3])
        pl.semaphore_signal(barrier, inc=1, device_id=partner, device_id_type=MESH)
        pl.semaphore_wait(barrier, 1)
        copy_to(wg_h, wq.at[:, 0, :, pl.ds(0, 128)], give_send.at[0], give_recv.at[0], partner)
        copy_to(wu_h, wq.at[:, 0, :, pl.ds(128, 128)], give_send.at[1], give_recv.at[1], partner)
        copy_to(cot_h, cot.at[0], give_send.at[2], give_recv.at[2], partner)
        for load in (load_xe, load_xl, load_gg, load_gu):
            load.start()

        arrived(dcat, share_recv.at[0])
        load_xe.wait()
        turned = jnp.transpose(dcat[...].astype(F32)).astype(BF16)
        for j in range(4):
            block = jnp.dot(turned, xe[:, 512 * j : 512 * j + 512], preferred_element_type=F32)
            for i in range(4):
                dwt[4 * j + i] = block[:, 128 * i : 128 * i + 128].astype(BF16)
        copy_to(dwt.at[f, pl.ds(256, 256)], dwr.at[0], dw_send.at[1], dw_recv.at[0], partner)
        for i in range(1, 16):
            to = (f + i) % 16
            for c in range(2):
                copy_to(
                    dwt.at[to, pl.ds(256 * c, 256)], dwr.at[i], dw_send.at[0], dw_recv.at[i],
                    {"fs": to, "tp": z * 2 + c},
                )

        load_xl.wait()
        arrived(wall, share_recv.at[1])
        both = jnp.dot(xl[...], wall[...], preferred_element_type=F32)
        gate, upv = both[:, 256:384], both[:, 384:]
        hid_other[...] = (gate * jax.nn.sigmoid(gate) * upv).astype(BF16)
        gate, upv = both[:, :128], both[:, 128:256]
        hid[...] = (gate * jax.nn.sigmoid(gate) * upv).astype(BF16)

        total = dwt[f, pl.ds(0, 256)].astype(F32)
        copy_to(hid_other, hid, hid_send, hid_recv, partner)
        for i in range(1, 16):
            arrived(dwr.at[i], dw_recv.at[i])
            total = total + dwr[i].astype(F32)
        new_gradients(total)

        for k in range(SUB):
            arrived(gi.at[:, at(k)], d2_recv.at[k])
        pltpu.make_async_copy(wg_h, wg_h, give_send.at[0]).wait()
        pltpu.make_async_copy(wu_h, wu_h, give_send.at[1]).wait()
        pltpu.make_async_copy(cot_h, cot_h, give_send.at[2]).wait()
        arrived(hid_other, hid_send)
        arrived(dwt.at[pl.ds(0, 15)], dw_send.at[0])
        arrived(dwr.at[0], dw_send.at[1])

    @pl.when(core == 1)
    def _():
        load_wg = pltpu.make_async_copy(wg_h, wq.at[:, 0, :, pl.ds(256, 128)], in_sem.at[3])
        load_wu = pltpu.make_async_copy(wu_h, wq.at[:, 0, :, pl.ds(384, 128)], in_sem.at[4])
        load_cot = pltpu.make_async_copy(cot_h, cot.at[1], in_sem.at[5])
        pl.semaphore_signal(barrier, inc=1, device_id=partner, device_id_type=MESH)
        for g in flips:
            pl.semaphore_signal(barrier, inc=1, device_id={"fs": g, "tp": t}, device_id_type=MESH)
        for by in (-2, -1, 1, 2):
            pl.semaphore_signal(barrier, inc=1, device_id=along(by), device_id_type=MESH)
        for load in (load_wg, load_wu, load_xe, load_cot, load_gg, load_gu):
            load.start()
        pl.semaphore_wait(barrier, 9)

        def gather_send(q, s, first, count):
            copy_to(
                wq.at[q, pl.ds(first, count)], wq.at[q, pl.ds(first + 2**s, count)],
                ag_send, ag_recv.at[q, s], {"fs": flips[(q + s) % 4], "tp": t},
            )

        def gather_wait(q, s):
            arrived(wq.at[q, pl.ds(2**s, 2**s)], ag_recv.at[q, s])

        load_wg.wait()
        load_wu.wait()
        arrived(wq.at[:, 0, :, pl.ds(0, 128)], give_recv.at[0])
        arrived(wq.at[:, 0, :, pl.ds(128, 128)], give_recv.at[1])
        for s in range(4):
            for q in range(4):
                gather_send(q, s, 0, 1)
        for a in range(3):
            for q in range(4):
                gather_wait(q, a)
                for s in range(a + 1, 4):
                    gather_send(q, s, 2**a, 2**a)
        for q in range(4):
            gather_wait(q, 3)
        for q in range(4):
            for i in range(16):
                bits = [(q + b) % 4 for b in range(4) if (i >> b) & 1]
                ox = x
                oy = y
                if 0 in bits:
                    ox = ox + 1 - 2 * (ox % 2)
                if 1 in bits:
                    ox = 3 - ox
                if 2 in bits:
                    oy = oy + 1 - 2 * (oy % 2)
                if 3 in bits:
                    oy = 3 - oy
                start = pl.multiple_of((oy * 4 + ox) * 128 + 32 * q, 32)
                wall[pl.ds(start, 32), :] = wq[q, i]

        load_xe.wait()
        load_cot.wait()
        arrived(cot.at[0], give_recv.at[2])
        both = jnp.dot(xe[...], wall[...], preferred_element_type=F32)
        for c in range(2):
            gate = both[:, 256 * c : 256 * c + 128]
            upv = both[:, 256 * c + 128 : 256 * c + 256]
            sigma = jax.nn.sigmoid(gate)
            cotangent = cot[c].astype(F32)
            delta_up = cotangent * gate * sigma
            delta_gate = cotangent * upv * sigma * (1.0 + gate * (1.0 - sigma))
            dcat[:, 256 * c : 256 * c + 128] = delta_gate.astype(BF16)
            dcat[:, 256 * c + 128 : 256 * c + 256] = delta_up.astype(BF16)
        for j in range(4):
            block = lax.dot_general(
                dcat[...], wall[512 * j : 512 * j + 512, :], (((1,), (1,)), ((), ())),
                preferred_element_type=F32,
            )
            for i in range(4):
                pc[4 * j + i] = block[:, 128 * i : 128 * i + 128]

        def chunk(by):
            return (z + nz + by) % nz

        def ring(k, w):
            go = 1 if (k + w) % 2 == 0 else -1
            return go, half - w

        def reduce_step(i, k, w):
            go, length = ring(k, w)
            far, near = half - 2 * i, half - 2 * i - 1
            if far > 0 and far <= length:
                value = pc[chunk(go * far), at(k)]
                if i > 0:
                    arrived(ring_r.at[w, 1, i - 1, at(k)], rs_recv.at[k, w, 1, i - 1])
                    value = value + ring_r[w, 1, i - 1, at(k)].astype(F32)
                    if far + 2 <= length:
                        arrived(ring_r.at[w, 0, i - 1, at(k)], rs_recv.at[k, w, 0, i - 1])
                        value = value + ring_r[w, 0, i - 1, at(k)].astype(F32)
                part = ring_s.at[w, 0, i, at(k)]
                ring_s[w, 0, i, at(k)] = value.astype(BF16)
                copy_to(
                    part, ring_r.at[w, 0, i, at(k)], rs_send, rs_recv.at[k, w, 0, i], along(2 * go)
                )
            if near > 0:
                part = ring_s.at[w, 1, i, at(k)]
                ring_s[w, 1, i, at(k)] = pc[chunk(go * near), at(k)].astype(BF16)
                copy_to(part, ring_r.at[w, 1, i, at(k)], rs_send, rs_recv.at[k, w, 1, i], along(go))

        sent = 0
        for i in range(steps):
            for k in range(SUB):
                for w in range(2):
                    reduce_step(i, k, w)
            if i == 0:
                copy_to(dcat, dcat, share_send.at[0], share_recv.at[0], partner)
                copy_to(wall, wall, share_send.at[1], share_recv.at[1], partner)

        def spread(i, k, w, origin):
            go, length = ring(k, w)
            part = gi.at[origin, at(k)]
            if 2 * i + 2 <= length:
                copy_to(part, part, gather_send_sem, gather_recv.at[k, w, 0, i], along(2 * go))
            if 2 * i + 1 <= length:
                copy_to(part, part, gather_send_sem, gather_recv.at[k, w, 1, i], along(go))

        for k in range(SUB):
            value = pc[z, at(k)]
            for w in range(2):
                for hop in range(2):
                    arrived(ring_r.at[w, hop, steps - 1, at(k)], rs_recv.at[k, w, hop, steps - 1])
                    value = value + ring_r[w, hop, steps - 1, at(k)].astype(F32)
            gi[z, at(k)] = value.astype(BF16)
            for w in range(2):
                spread(0, k, w, z)
            copy_to(gi.at[z, at(k)], gi.at[z, at(k)], d2_send, d2_recv.at[k], partner)

        for i in range(steps):
            if i == steps - 1:
                total = jnp.zeros((256, 128), F32)
                for j in range(16):
                    arrived(dwr.at[j], dw_recv.at[j])
                    total = total + dwr[j].astype(F32)
                new_gradients(total)
            for k in range(SUB):
                for w in range(2):
                    go, length = ring(k, w)
                    if 2 * i + 1 <= length:
                        origin = chunk(-go * (2 * i + 1))
                        part = gi.at[origin, at(k)]
                        arrived(part, gather_recv.at[k, w, 1, i])
                        copy_to(part, part, d2_send, d2_recv.at[k], partner)
                    if 2 * i + 2 <= length:
                        origin = chunk(-go * (2 * i + 2))
                        part = gi.at[origin, at(k)]
                        arrived(part, gather_recv.at[k, w, 0, i])
                        if i + 1 < steps:
                            spread(i + 1, k, w, origin)
                        copy_to(part, part, d2_send, d2_recv.at[k], partner)

        arrived(hid, hid_recv)
        arrived(dcat, share_send.at[0])
        arrived(wall, share_send.at[1])
        arrived(wq.at[:, pl.ds(0, 15)], ag_send)
        arrived(gi, d2_send)
        arrived(gi.at[pl.ds(0, nz - 1)], rs_send)
        arrived(gi.at[pl.ds(0, nz - 1)], gather_send_sem)


def store(hid, gi, ngg, ngu, hid_o, gi_o, ngg_o, ngu_o, hid_sem, gi_sem, ngg_sem, ngu_sem):
    for o in range(gi.shape[0]):
        pltpu.make_async_copy(gi.at[o], gi_o.at[:, pl.ds(o * 128, 128)], gi_sem).start()
    small = [
        pltpu.make_async_copy(hid, hid_o, hid_sem),
        pltpu.make_async_copy(ngg, ngg_o, ngg_sem),
        pltpu.make_async_copy(ngu, ngu_o, ngu_sem),
    ]
    for copy in small:
        copy.start()
    for copy in small:
        copy.wait()
    pltpu.make_async_copy(gi, gi, gi_sem).wait()


def per_device(nz, x_later, x_earlier, cot_hidden, w_gate, w_up, grad_gate, grad_up):
    rows, width = x_later.shape
    steps = nz // 4
    dma = pltpu.SemaphoreType.DMA
    vmem = pltpu.VMEM
    hid, gi, ngg, ngu = pl.pallas_call(
        functools.partial(kernel, nz),
        out_shape=(
            vmem((rows, 128), BF16),
            vmem((nz, rows, 128), BF16),
            vmem((128, 128), F32),
            vmem((128, 128), F32),
        ),
        in_specs=[pl.BlockSpec(memory_space=pl.ANY)] * 7,
        out_specs=(pl.BlockSpec(memory_space=vmem),) * 4,
        scratch_shapes=[
            vmem((rows, width), BF16),
            vmem((rows, width), BF16),
            vmem((2, rows, 128), BF16),
            vmem((128, 128), F32),
            vmem((128, 128), F32),
            vmem((4, 16, 32, 512), BF16),
            vmem((width, 512), BF16),
            vmem((rows, 512), BF16),
            vmem((16, 512, 128), BF16),
            vmem((16, 256, 128), BF16),
            vmem((rows, 128), BF16),
            vmem((nz, rows, 128), F32),
            vmem((2, 2, steps, rows, 128), BF16),
            vmem((2, 2, steps, rows, 128), BF16),
            dma((6,)),
            dma((3,)),
            dma((3,)),
            dma,
            dma((4, 4)),
            dma((2,)),
            dma((2,)),
            dma((2,)),
            dma((16,)),
            dma,
            dma,
            dma,
            dma((SUB, 2, 2, steps)),
            dma,
            dma((SUB, 2, 2, steps)),
            dma,
            dma((SUB,)),
        ],
        compiler_params=pltpu.CompilerParams(
            collective_id=0, has_side_effects=True, vmem_limit_bytes=48 * 1024 * 1024
        ),
        name="step",
    )(
        *(
            pltpu.with_memory_space_constraint(operand, pltpu.HBM)
            for operand in (
                x_later,
                x_earlier,
                cot_hidden,
                w_gate.reshape(4, 32, 128),
                w_up.reshape(4, 32, 128),
                grad_gate,
                grad_up,
            )
        )
    )
    any_spec = pl.BlockSpec(memory_space=pl.ANY)
    return pl.pallas_call(
        store,
        out_shape=(
            jax.ShapeDtypeStruct((rows, 128), BF16),
            jax.ShapeDtypeStruct((rows, width), BF16),
            jax.ShapeDtypeStruct((128, 128), F32),
            jax.ShapeDtypeStruct((128, 128), F32),
        ),
        in_specs=[pl.BlockSpec(memory_space=vmem)] * 4,
        out_specs=(any_spec,) * 4,
        scratch_shapes=[dma, dma, dma, dma],
        name="store",
    )(*(pltpu.with_memory_space_constraint(r, vmem) for r in (hid, gi, ngg, ngu)))


def solution(mesh):
    placed = (
        P("fs", None),
        P("fs", None),
        P("fs", "tp"),
        P("fs", "tp"),
        P("fs", "tp"),
        P("fs", "tp"),
        P("fs", "tp"),
    )
    return jax.shard_map(
        functools.partial(per_device, mesh.shape["tp"] // 2),
        mesh=mesh,
        in_specs=placed,
        out_specs=(P("fs", "tp"), P("fs", None), P("fs", "tp"), P("fs", "tp")),
        check_vma=False,
    )
```

time: 243 us -> 62.7 us (0.26)
  blocking collectives: 113 us -> 0 us
  waiting for transfers between devices: 65.4 us -> 0 us
  Pallas kernels: 0 us -> 62 us
  starting transfers between devices: 28.9 us -> 0 us
  between operations: 16.5 us -> 0.64 us
  local copies, waits for them, and re-layouts: 11.4 us -> 0 us
  matrix products: 7.43 us -> 0 us
    unnamed x1 -> x0, blocking collectives: 74.8 us -> none
    all_gather x1 -> x0, waiting for transfers between devices: 65.4 us -> none  [per_device(): grad_input = lax.all_gather(grad_share, 'tp', axis=0, tiled=True)]
    pallas_call x0 -> x2, Pallas kernels: none -> 62 us  [the longest x1 60.7 us: per_device(): pl.pallas_call(functools.partial(kernel, nz), out_shape=(vmem((rows, 128)...]
    all_gather x2 -> x0, blocking collectives: 38 us -> none  [the longest x1 20.1 us: per_device(): lax.all_gather(w_up, 'fs', axis=0, tiled=True)]
    unnamed x9 -> x0, starting transfers between devices: 28.9 us -> none
    unnamed x31 -> x0, local copies, waits for them, and re-layouts: 11.4 us -> none
    dot_general x7 -> x0, matrix products: 7.43 us -> none  [the longest x1 2.09 us: per_device(): jnp.dot(x_later, whole_gate, preferred_element_type=jnp.float32)]
  transfers between devices with their start and end apart: 10 -> 0, of which waited for: 1 -> 0; matrix products, arithmetic and copies ran while one was open for 35% -> 0% of each run, Pallas kernels for 0% -> 0%
where the time goes in v2:
time: 62.7 us; the launch traced here: 62.6 us
  Pallas kernels  62 us (99%)
  between operations  0.64 us (1%)
    pallas_call x1, Pallas kernels, per_device(): pl.pallas_call(functools.partial(kernel, nz), out_shape=(vmem((rows, 128)...  60.7 us

profile of v2, /device:TPU:1, one launch (start us, length us, event | category | flops | bytes accessed | tf_op | source)
XLA Modules:
  0.0 62.6 jit_solution(10422070185839718233)
XLA Ops:
  0.6 60.7 %step.1 = (bf16[384,128]{1,0:T(8,128)(2,1)S(1)}, bf16[16,384,128]{2,1,0:T(8,128)(2,1)S(1)}, f32[128,128]{1,0:T(8,128)S(1)}, f32[128,128]{1,0:T(8,128)S(1)}) custom-call(bf16[384,2048]{1,0:T(8,128)(2,1)} %xl_h.1, bf16[384,2048]{1,0:T(8,128)(2,1)} %xe_h.1, bf16[384,128]{1,0:T(8,128)(2,1)} %cot_h.1, bf16[4,32,128]{2,1,0:T(8,128)(2,1)} %bitcast.2, ...), custom_call_target="tpu_custom_call" | custom-call | tf_op jit(solution)/shard_map/step/pallas_call | solution.py:302
  61.4 1.2 %store.1 = (bf16[384,128]{1,0:T(8,128)(2,1)}, bf16[384,2048]{1,0:T(8,128)(2,1)}, f32[128,128]{1,0:T(8,128)}, f32[128,128]{1,0:T(8,128)}) custom-call(bf16[384,128]{1,0:T(8,128)(2,1)S(1)} %get-tuple-element.8.hid, bf16[16,384,128]{2,1,0:T(8,128)(2,1)S(1)} %get-tuple-element.9.gi, f32[128,128]{1,0:T(8,128)S(1)} %get-tuple-element.10.ngg, ...), custom_call_target="tpu_custom_call" | custom-call | tf_op jit(solution)/shard_map/store/pallas_call | solution.py:364

commit v3 on v2

v3 whole, which is shorter than its diff:
```python
import functools

import jax
import jax.numpy as jnp
from jax import lax
from jax.experimental import pallas as pl
from jax.experimental.pallas import tpu as pltpu
from jax.sharding import PartitionSpec as P

MESH = pl.DeviceIdType.MESH
SUB = 4
DOWN = (8, 6, 4, 2, 0)
UP = (0, 2, 4, 6, 8)
F32 = jnp.float32
BF16 = jnp.bfloat16


def copy_to(src, dst, send_sem, recv_sem, who):
    pltpu.make_async_remote_copy(
        src_ref=src, dst_ref=dst, send_sem=send_sem, recv_sem=recv_sem,
        device_id=who, device_id_type=MESH,
    ).start()


def arrived(ref, sem):
    pltpu.make_async_copy(ref, ref, sem).wait()


def between(stops):
    return [n for n in range(len(stops) - 1) if abs(stops[n] - stops[n + 1]) == 2]


def kernel(
    nz,
    xl_h, xe_h, cot_h, wg_h, wu_h, gg_h, gu_h, hid, gi, ngg, ngu,
    xl, xe, cot, wst, gg, gu,
    wq, wall,
    dcat, dwt, dwr, hid_other,
    pc, ring_s, ring_r,
    in_sem, give_send, give_recv, ag_send, ag_recv,
    share_send, share_recv, dw_send, dw_recv, hid_send, hid_recv,
    rs_send, rs_recv, out_send, out_recv, out_side_recv, d2_send, d2_recv,
):
    rows = xe.shape[0]
    piece = rows // SUB

    f = lax.axis_index("fs")
    t = lax.axis_index("tp")
    y, x = f // 4, f % 4
    z, core = t // 2, t % 2
    x1 = x + 1 - 2 * (x % 2)
    y1 = y + 1 - 2 * (y % 2)
    flips = [y * 4 + x1, y * 4 + (3 - x), y1 * 4 + x, (3 - y) * 4 + x]
    partner = {"fs": f, "tp": z * 2 + 1 - core}

    def across(d, c):
        return {"fs": flips[d % 4], "tp": z * 2 + c}

    def along(by):
        return {"fs": f, "tp": ((z + nz + by) % nz) * 2 + core}

    def at(k):
        return pl.ds(k * piece, piece)

    load_xe = pltpu.make_async_copy(xe_h, xe, in_sem.at[0])
    load_gg = pltpu.make_async_copy(gg_h, gg, in_sem.at[1])
    load_gu = pltpu.make_async_copy(gu_h, gu, in_sem.at[2])
    barrier = pltpu.get_barrier_semaphore()

    def greet(who):
        pl.semaphore_signal(barrier, inc=1, device_id=who, device_id_type=MESH)

    def new_gradients(total):
        load_gg.wait()
        load_gu.wait()
        ngg[...] = gg[...] + jnp.transpose(total[:128])
        ngu[...] = gu[...] + jnp.transpose(total[128:])

    waves = [(1, 1), (2, 1), (3, 1), (4, 2), (6, 2), (8, 8)]

    def wave_of(slot):
        return max(n for n in range(6) if waves[n][0] <= slot)

    @pl.when(core == 0)
    def _():
        load_wg = pltpu.make_async_copy(wg_h, wst.at[0], in_sem.at[3])
        load_wu = pltpu.make_async_copy(wu_h, wst.at[1], in_sem.at[4])
        load_xl = pltpu.make_async_copy(xl_h, xl, in_sem.at[5])
        greet(partner)
        for d in range(4):
            greet(across(d, 1))
        load_wg.start()
        load_wu.start()
        pl.semaphore_wait(barrier, 5)
        load_wg.wait()
        load_wu.wait()
        for s in range(4):
            for q in range(2):
                copy_to(
                    wst.at[q], wq.at[q, 2**s], give_send.at[0], ag_recv.at[wave_of(2**s)],
                    across(q + s, 1),
                )
        for q in range(2):
            copy_to(wst.at[q], wq.at[q, 0], give_send.at[0], give_recv.at[q], partner)
        copy_to(cot_h, cot.at[0], give_send.at[1], give_recv.at[2], partner)
        for load in (load_xe, load_xl, load_gg, load_gu):
            load.start()

        arrived(dcat, share_recv.at[0])
        load_xe.wait()
        turned = jnp.transpose(dcat[...].astype(F32)).astype(BF16)
        for j in range(4):
            block = jnp.dot(turned, xe[:, 512 * j : 512 * j + 512], preferred_element_type=F32)
            for i in range(4):
                dwt[4 * j + i] = block[:, 128 * i : 128 * i + 128].astype(BF16)
        copy_to(dwt.at[f, pl.ds(256, 256)], dwr.at[0], dw_send.at[1], dw_recv, partner)
        for i in range(1, 16):
            to = (f + i) % 16
            for c in range(2):
                copy_to(
                    dwt.at[to, pl.ds(256 * c, 256)], dwr.at[i], dw_send.at[0], dw_recv,
                    {"fs": to, "tp": z * 2 + c},
                )

        load_xl.wait()
        arrived(wall, share_recv.at[1])
        both = jnp.dot(xl[...], wall[...], preferred_element_type=F32)
        gate, upv = both[:, 256:384], both[:, 384:]
        hid_other[...] = (gate * jax.nn.sigmoid(gate) * upv).astype(BF16)
        gate, upv = both[:, :128], both[:, 128:256]
        hid[...] = (gate * jax.nn.sigmoid(gate) * upv).astype(BF16)

        total = dwt[f, pl.ds(0, 256)].astype(F32)
        copy_to(hid_other, hid, hid_send, hid_recv, partner)
        arrived(dwr.at[pl.ds(1, 15)], dw_recv)
        for i in range(1, 16):
            total = total + dwr[i].astype(F32)
        new_gradients(total)

        arrived(gi, d2_recv)
        arrived(wq.at[0, pl.ds(0, 10)], give_send.at[0])
        pltpu.make_async_copy(cot_h, cot_h, give_send.at[1]).wait()
        arrived(hid_other, hid_send)
        arrived(dwt.at[pl.ds(0, 15)], dw_send.at[0])
        arrived(dwr.at[0], dw_send.at[1])

    @pl.when(core == 1)
    def _():
        load_wg = pltpu.make_async_copy(wg_h, wq.at[2, 0], in_sem.at[3])
        load_wu = pltpu.make_async_copy(wu_h, wq.at[3, 0], in_sem.at[4])
        load_cot = pltpu.make_async_copy(cot_h, cot.at[1], in_sem.at[5])
        greet(partner)
        for d in range(4):
            greet(across(d, 0))
            greet(across(d, 1))
        for by in (-2, -1, 1, 2):
            greet(along(by))
        for load in (load_wg, load_wu, load_xe, load_cot, load_gg, load_gu):
            load.start()
        pl.semaphore_wait(barrier, 13)

        def gather_send(q, s, first, count):
            copy_to(
                wq.at[q, pl.ds(first, count)], wq.at[q, pl.ds(first + 2**s, count)],
                ag_send, ag_recv.at[wave_of(first + 2**s)], across(q + s, 1),
            )

        def gather_wait(n):
            arrived(wq.at[:, pl.ds(waves[n][0], waves[n][1])], ag_recv.at[n])

        def in_order(first, count):
            for q in range(4):
                for i in range(first, first + count):
                    bits = [(q + b) % 4 for b in range(4) if (i >> b) & 1]
                    ox = x
                    oy = y
                    if 0 in bits:
                        ox = ox + 1 - 2 * (ox % 2)
                    if 1 in bits:
                        ox = 3 - ox
                    if 2 in bits:
                        oy = oy + 1 - 2 * (oy % 2)
                    if 3 in bits:
                        oy = 3 - oy
                    start = pl.multiple_of((oy * 4 + ox) * 128, 128)
                    wall[pl.ds(start, 128), 128 * q : 128 * q + 128] = wq[q, i]

        load_wg.wait()
        load_wu.wait()
        for s in range(4):
            for q in (2, 3):
                gather_send(q, s, 0, 1)
        for n in range(5):
            gather_wait(n)
            first, count = waves[n]
            for s in range(first.bit_length(), 4):
                for q in range(4):
                    gather_send(q, s, first, count)
        for q in range(2):
            arrived(wq.at[q, 0], give_recv.at[q])
        in_order(0, 8)
        gather_wait(5)
        in_order(8, 8)

        load_xe.wait()
        load_cot.wait()
        arrived(cot.at[0], give_recv.at[2])
        both = jnp.dot(xe[...], wall[...], preferred_element_type=F32)
        for c in range(2):
            gate = both[:, 256 * c : 256 * c + 128]
            upv = both[:, 256 * c + 128 : 256 * c + 256]
            sigma = jax.nn.sigmoid(gate)
            cotangent = cot[c].astype(F32)
            delta_up = cotangent * gate * sigma
            delta_gate = cotangent * upv * sigma * (1.0 + gate * (1.0 - sigma))
            dcat[:, 256 * c : 256 * c + 128] = delta_gate.astype(BF16)
            dcat[:, 256 * c + 128 : 256 * c + 256] = delta_up.astype(BF16)

        def chunk(by):
            return (z + nz + by) % nz

        def partials(offsets):
            rhs = jnp.concatenate(
                [wall[pl.ds(pl.multiple_of(chunk(by) * 128, 128), 128), :] for by in offsets], 0
            )
            block = lax.dot_general(
                dcat[...], rhs, (((1,), (1,)), ((), ())), preferred_element_type=F32
            )
            for i, by in enumerate(offsets):
                pc[by % nz] = block[:, 128 * i : 128 * i + 128]

        ways = (1, -1)

        def length(k, w):
            return 8 if (k + w) % 2 == 0 else 7

        def gathered(value, n, k, w):
            first = 0 if n > 0 and DOWN[n - 1] <= length(k, w) else 1
            count = 2 if n - 1 in between(DOWN) else 1
            if first < count:
                part = ring_r.at[w, n - 1, k, pl.ds(first, count - first)]
                arrived(part, rs_recv.at[k, w, n - 1])
                for kind in range(first, count):
                    value = value + ring_r[w, n - 1, k, kind].astype(F32)
            return value

        def reduce_send(value, n, k, w, kind, hops):
            ring_s[w, n, k, kind] = value.astype(BF16)
            copy_to(
                ring_s.at[w, n, k, kind], ring_r.at[w, n, k, kind],
                rs_send, rs_recv.at[k, w, n], along(ways[w] * hops),
            )

        def reduce_stop(n):
            for k in range(SUB):
                for w in range(2):
                    if DOWN[n] <= length(k, w):
                        value = gathered(pc[ways[w] * DOWN[n] % nz, at(k)], n, k, w)
                        reduce_send(value, n, k, w, 0, DOWN[n] - DOWN[n + 1])
                    if n in between(DOWN):
                        reduce_send(pc[ways[w] * (DOWN[n] - 1) % nz, at(k)], n, k, w, 1, 1)

        partials((8, 7, -7, 6))
        reduce_stop(0)
        partials((-6, 5, -5, 4))
        partials((-4, 3, -3, 2))
        partials((-2, 1, -1, 0))
        copy_to(dcat, dcat, share_send.at[0], share_recv.at[0], partner)
        copy_to(wall, wall, share_send.at[1], share_recv.at[1], partner)
        for n in range(1, len(DOWN) - 1):
            reduce_stop(n)

        def spread(n, k, w, origin):
            part = gi.at[origin, at(k)]
            if n + 1 < len(UP) and UP[n + 1] <= length(k, w):
                copy_to(part, part, out_send, out_recv.at[k, w, n], along(ways[w] * (UP[n + 1] - UP[n])))
            if n in between(UP):
                j = between(UP).index(n)
                copy_to(part, part, out_send, out_side_recv.at[w, j], along(ways[w]))

        def to_partner(part):
            copy_to(part, part, d2_send, d2_recv, partner)

        for k in range(SUB):
            value = pc[0, at(k)]
            for w in range(2):
                value = gathered(value, len(DOWN) - 1, k, w)
            gi[z, at(k)] = value.astype(BF16)
            for w in range(2):
                spread(0, k, w, z)
        to_partner(gi.at[z])

        for n in range(len(UP) - 1):
            for k in range(SUB):
                for w in range(2):
                    if UP[n + 1] <= length(k, w):
                        origin = chunk(-ways[w] * UP[n + 1])
                        arrived(gi.at[origin, at(k)], out_recv.at[k, w, n])
                        spread(n + 1, k, w, origin)
                        to_partner(gi.at[origin, at(k)])
            if n in between(UP):
                j = between(UP).index(n)
                for w in range(2):
                    origin = chunk(-ways[w] * (UP[n] + 1))
                    arrived(gi.at[origin], out_side_recv.at[w, j])
                    to_partner(gi.at[origin])
            if n == len(UP) - 3:
                total = jnp.zeros((256, 128), F32)
                arrived(dwr, dw_recv)
                for j in range(16):
                    total = total + dwr[j].astype(F32)
                new_gradients(total)

        arrived(hid, hid_recv)
        arrived(dcat, share_send.at[0])
        arrived(wall, share_send.at[1])
        arrived(wq.at[:, pl.ds(0, 13)], ag_send)
        arrived(gi, d2_send)
        arrived(gi.at[pl.ds(0, nz - 1)], rs_send)
        arrived(gi.at[pl.ds(0, nz - 1)], out_send)


def store(hid, gi, ngg, ngu, hid_o, gi_o, ngg_o, ngu_o, hid_sem, gi_sem, ngg_sem, ngu_sem):
    for o in range(gi.shape[0]):
        pltpu.make_async_copy(gi.at[o], gi_o.at[:, pl.ds(o * 128, 128)], gi_sem).start()
    small = [
        pltpu.make_async_copy(hid, hid_o, hid_sem),
        pltpu.make_async_copy(ngg, ngg_o, ngg_sem),
        pltpu.make_async_copy(ngu, ngu_o, ngu_sem),
    ]
    for copy in small:
        copy.start()
    for copy in small:
        copy.wait()
    pltpu.make_async_copy(gi, gi, gi_sem).wait()


def per_device(nz, x_later, x_earlier, cot_hidden, w_gate, w_up, grad_gate, grad_up):
    rows, width = x_later.shape
    dma = pltpu.SemaphoreType.DMA
    vmem = pltpu.VMEM
    hid, gi, ngg, ngu = pl.pallas_call(
        functools.partial(kernel, nz),
        out_shape=(
            vmem((rows, 128), BF16),
            vmem((nz, rows, 128), BF16),
            vmem((128, 128), F32),
            vmem((128, 128), F32),
        ),
        in_specs=[pl.BlockSpec(memory_space=pl.ANY)] * 7,
        out_specs=(pl.BlockSpec(memory_space=vmem),) * 4,
        scratch_shapes=[
            vmem((rows, width), BF16),
            vmem((rows, width), BF16),
            vmem((2, rows, 128), BF16),
            vmem((2, 128, 128), BF16),
            vmem((128, 128), F32),
            vmem((128, 128), F32),
            vmem((4, 16, 128, 128), BF16),
            vmem((width, 512), BF16),
            vmem((rows, 512), BF16),
            vmem((16, 512, 128), BF16),
            vmem((16, 256, 128), BF16),
            vmem((rows, 128), BF16),
            vmem((nz, rows, 128), F32),
            vmem((2, len(DOWN) - 1, SUB, 2, rows // SUB, 128), BF16),
            vmem((2, len(DOWN) - 1, SUB, 2, rows // SUB, 128), BF16),
            dma((6,)),
            dma((2,)),
            dma((3,)),
            dma,
            dma((6,)),
            dma((2,)),
            dma((2,)),
            dma((2,)),
            dma,
            dma,
            dma,
            dma,
            dma((SUB, 2, len(DOWN) - 1)),
            dma,
            dma((SUB, 2, len(UP) - 1)),
            dma((2, max(1, len(between(UP))))),
            dma,
            dma,
        ],
        compiler_params=pltpu.CompilerParams(
            collective_id=0, has_side_effects=True, vmem_limit_bytes=48 * 1024 * 1024
        ),
        name="step",
    )(
        *(
            pltpu.with_memory_space_constraint(operand, pltpu.HBM)
            for operand in (
                x_later,
                x_earlier,
                cot_hidden,
                w_gate,
                w_up,
                grad_gate,
                grad_up,
            )
        )
    )
    any_spec = pl.BlockSpec(memory_space=pl.ANY)
    return pl.pallas_call(
        store,
        out_shape=(
            jax.ShapeDtypeStruct((rows, 128), BF16),
            jax.ShapeDtypeStruct((rows, width), BF16),
            jax.ShapeDtypeStruct((128, 128), F32),
            jax.ShapeDtypeStruct((128, 128), F32),
        ),
        in_specs=[pl.BlockSpec(memory_space=vmem)] * 4,
        out_specs=(any_spec,) * 4,
        scratch_shapes=[dma, dma, dma, dma],
        name="store",
    )(*(pltpu.with_memory_space_constraint(r, vmem) for r in (hid, gi, ngg, ngu)))


def solution(mesh):
    placed = (
        P("fs", None),
        P("fs", None),
        P("fs", "tp"),
        P("fs", "tp"),
        P("fs", "tp"),
        P("fs", "tp"),
        P("fs", "tp"),
    )
    return jax.shard_map(
        functools.partial(per_device, mesh.shape["tp"] // 2),
        mesh=mesh,
        in_specs=placed,
        out_specs=(P("fs", "tp"), P("fs", None), P("fs", "tp"), P("fs", "tp")),
        check_vma=False,
    )
```

time: 62.7 us -> 58 us (0.925)
  Pallas kernels: 62 us -> 57.2 us
    pallas_call x1, Pallas kernels: 60.7 us -> 56 us  [per_device(): pl.pallas_call(functools.partial(kernel, nz), out_shape=(vmem((rows, 128)...]
where the time goes in v3:
time: 58 us; the launch traced here: 57.9 us
  Pallas kernels  57.2 us (99%)
  between operations  0.64 us (1%)
    pallas_call x1, Pallas kernels, per_device(): pl.pallas_call(functools.partial(kernel, nz), out_shape=(vmem((rows, 128)...  56 us
    pallas_call x1, Pallas kernels, per_device(): pl.pallas_call(store, out_shape=(jax.ShapeDtypeStruct((rows, 128), BF16),...  1.24 us

profile of v3, /device:TPU:1, one launch (start us, length us, event | category | flops | bytes accessed | tf_op | source)
XLA Modules:
  0.0 57.9 jit_solution(10090015607621685241)
XLA Ops:
  0.6 56.0 %step.1 = (bf16[384,128]{1,0:T(8,128)(2,1)S(1)}, bf16[16,384,128]{2,1,0:T(8,128)(2,1)S(1)}, f32[128,128]{1,0:T(8,128)S(1)}, f32[128,128]{1,0:T(8,128)S(1)}) custom-call(bf16[384,2048]{1,0:T(8,128)(2,1)} %xl_h.1, bf16[384,2048]{1,0:T(8,128)(2,1)} %xe_h.1, bf16[384,128]{1,0:T(8,128)(2,1)} %cot_h.1, bf16[128,128]{1,0:T(8,128)(2,1)} %wg_h.1, ...), custom_call_target="tpu_custom_call" | custom-call | tf_op jit(solution)/shard_map/step/pallas_call | solution.py:342
  56.6 1.2 %store.1 = (bf16[384,128]{1,0:T(8,128)(2,1)}, bf16[384,2048]{1,0:T(8,128)(2,1)}, f32[128,128]{1,0:T(8,128)}, f32[128,128]{1,0:T(8,128)}) custom-call(bf16[384,128]{1,0:T(8,128)(2,1)S(1)} %get-tuple-element.8.hid, bf16[16,384,128]{2,1,0:T(8,128)(2,1)S(1)} %get-tuple-element.9.gi, f32[128,128]{1,0:T(8,128)S(1)} %get-tuple-element.10.ngg, ...), custom_call_target="tpu_custom_call" | custom-call | tf_op jit(solution)/shard_map/store/pallas_call | solution.py:406

commit v4 on v3

v4 whole, which is shorter than its diff:
```python
import functools

import jax
import jax.numpy as jnp
from jax import lax
from jax.experimental import pallas as pl
from jax.experimental.pallas import tpu as pltpu
from jax.sharding import PartitionSpec as P

MESH = pl.DeviceIdType.MESH
SUB = 6
DOWN = (8, 6, 4, 2, 0)
UP = (0, 2, 4, 6, 8)
F32 = jnp.float32
BF16 = jnp.bfloat16


def copy_to(src, dst, send_sem, recv_sem, who):
    pltpu.make_async_remote_copy(
        src_ref=src, dst_ref=dst, send_sem=send_sem, recv_sem=recv_sem,
        device_id=who, device_id_type=MESH,
    ).start()


def arrived(ref, sem):
    pltpu.make_async_copy(ref, ref, sem).wait()


def between(stops):
    return [n for n in range(len(stops) - 1) if abs(stops[n] - stops[n + 1]) == 2]


def kernel(
    nz,
    xl_h, xe_h, cot_h, wg_h, wu_h, gg_h, gu_h, hid, gi, ngg, ngu,
    xl, xe, cot, wst, grads, grads_other,
    wq,
    dcat, dwt, dwr, hid_other,
    pc, ring_s, ring_r,
    in_sem, give_send, give_recv, ag_send, first_recv, second_recv,
    share_send, share_recv, dw_send, dw_recv, hid_send, hid_recv,
    grads_send, grads_recv, new_recv,
    rs_send, rs_recv, out_send, out_recv, out_side_recv, d2_send, d2_recv,
):
    rows = xe.shape[0]
    piece = rows // SUB

    f = lax.axis_index("fs")
    t = lax.axis_index("tp")
    y, x = f // 4, f % 4
    z, core = t // 2, t % 2
    partner = {"fs": f, "tp": z * 2 + 1 - core}

    def beside(d, by, c):
        place = (y * 4 + (x + by) % 4, (y + by) % 4 * 4 + x)[d]
        return {"fs": place, "tp": z * 2 + c}

    def along(by):
        return {"fs": f, "tp": ((z + nz + by) % nz) * 2 + core}

    def at(k):
        return pl.ds(k * piece, piece)

    load_xe = pltpu.make_async_copy(xe_h, xe, in_sem.at[0])
    barrier = pltpu.get_barrier_semaphore()

    def greet(who):
        pl.semaphore_signal(barrier, inc=1, device_id=who, device_id_type=MESH)

    def weights():
        return jnp.concatenate([wq[q].reshape(16 * 128, 128) for q in range(4)], 1)

    @pl.when(core == 0)
    def _():
        load_wg = pltpu.make_async_copy(wg_h, wst.at[0], in_sem.at[3])
        load_wu = pltpu.make_async_copy(wu_h, wst.at[1], in_sem.at[4])
        load_xl = pltpu.make_async_copy(xl_h, xl, in_sem.at[5])
        load_gg = pltpu.make_async_copy(gg_h, grads.at[0], in_sem.at[1])
        load_gu = pltpu.make_async_copy(gu_h, grads.at[1], in_sem.at[2])
        greet(partner)
        load_wg.start()
        load_wu.start()
        pl.semaphore_wait(barrier, 4)
        load_wg.wait()
        load_wu.wait()
        mine = wq.at[pl.ds(0, 2), f]
        for by in (2, 1, 3):
            copy_to(wst, mine, give_send.at[0], first_recv.at[0, by - 1], beside(0, by, 1))
        copy_to(wst, mine, give_send.at[0], give_recv.at[0], partner)
        copy_to(cot_h, cot.at[0], give_send.at[1], give_recv.at[1], partner)
        for load in (load_xe, load_xl, load_gg, load_gu):
            load.start()

        arrived(dcat, share_recv.at[0])
        load_xe.wait()
        turned = jnp.transpose(dcat[...].astype(F32)).astype(BF16)
        for j in range(4):
            block = jnp.dot(turned, xe[:, 512 * j : 512 * j + 512], preferred_element_type=F32)
            for i in range(4):
                dwt[4 * j + i] = block[:, 128 * i : 128 * i + 128].astype(BF16)
        for i in range(1, 16):
            to = (f + i) % 16
            copy_to(
                dwt.at[to], dwr.at[i - 1], dw_send, dw_recv, {"fs": to, "tp": z * 2}
            )

        load_xl.wait()
        arrived(wq, share_recv.at[1])
        both = jnp.dot(xl[...], weights(), preferred_element_type=F32)
        gate, upv = both[:, 256:384], both[:, 384:]
        hid_other[...] = (gate * jax.nn.sigmoid(gate) * upv).astype(BF16)
        gate, upv = both[:, :128], both[:, 128:256]
        hid[...] = (gate * jax.nn.sigmoid(gate) * upv).astype(BF16)

        copy_to(hid_other, hid, hid_send, hid_recv, partner)

        total = dwt[f].astype(F32)
        arrived(dwr, dw_recv)
        for i in range(15):
            total = total + dwr[i].astype(F32)
        arrived(grads.at[pl.ds(2, 2)], grads_recv)
        for i in range(2):
            grads_other[i] = grads[2 + i] + jnp.transpose(total[256 + 128 * i : 384 + 128 * i])
        load_gg.wait()
        load_gu.wait()
        ngg[...] = grads[0] + jnp.transpose(total[:128])
        ngu[...] = grads[1] + jnp.transpose(total[128:256])
        copy_to(grads_other.at[0], ngg, grads_send, new_recv.at[0], partner)
        copy_to(grads_other.at[1], ngu, grads_send, new_recv.at[1], partner)

        arrived(gi, d2_recv)
        arrived(wq.at[pl.ds(0, 2), pl.ds(0, 4)], give_send.at[0])
        pltpu.make_async_copy(cot_h, cot_h, give_send.at[1]).wait()
        arrived(hid_other, hid_send)
        arrived(dwr, dw_send)
        arrived(grads_other, grads_send)

    @pl.when(core == 1)
    def _():
        load_wg = pltpu.make_async_copy(wg_h, wq.at[2, f], in_sem.at[3])
        load_wu = pltpu.make_async_copy(wu_h, wq.at[3, f], in_sem.at[4])
        load_cot = pltpu.make_async_copy(cot_h, cot.at[1], in_sem.at[5])
        greet(partner)
        for by in (1, 2, 3):
            greet(beside(0, by, 0))
            greet(beside(1, by, 1))
        for by in (-2, -1, 1, 2):
            greet(along(by))
        for load in (load_wg, load_wu, load_xe, load_cot):
            load.start()
        pl.semaphore_wait(barrier, 8)

        def block(d, by):
            place = (y * 4 + (x + 4 - by) % 4, (y + 4 - by) % 4 * 4 + x)[d]
            return wq.at[pl.ds(2 * d, 2), place]

        def pass_on(part, d, offsets=(2, 1, 3)):
            for by in offsets:
                copy_to(part, part, ag_send.at[1], second_recv, beside(d, by, 1))

        def come(d, by):
            part = block(d, by)
            arrived(part, first_recv.at[d, by - 1])
            return part

        load_wg.wait()
        load_wu.wait()
        mine = wq.at[pl.ds(2, 2), f]
        for by in (2, 1, 3):
            copy_to(mine, mine, ag_send.at[0], first_recv.at[1, by - 1], beside(1, by, 1))
        arrived(wq.at[pl.ds(0, 2), f], give_recv.at[0])
        pass_on(wq.at[pl.ds(0, 2), f], 1)
        for by in (1, 3):
            pass_on(come(0, by), 1)
            pass_on(mine, 0, (4 - by,))
        for by in (1, 3):
            pass_on(come(1, by), 0, (1, 3))
        pass_on(come(0, 2), 1)
        for part in (mine, block(1, 1), block(1, 3)):
            pass_on(part, 0, (2,))
        pass_on(come(1, 2), 0)
        arrived(wq.at[:, pl.ds(0, 12)], second_recv)

        load_xe.wait()
        load_cot.wait()
        arrived(cot.at[0], give_recv.at[1])
        def deltas(rs):
            both = jnp.dot(xe[rs, :], weights(), preferred_element_type=F32)
            for c in range(2):
                gate = both[:, 256 * c : 256 * c + 128]
                upv = both[:, 256 * c + 128 : 256 * c + 256]
                sigma = jax.nn.sigmoid(gate)
                cotangent = cot[c, rs].astype(F32)
                delta_up = cotangent * gate * sigma
                delta_gate = cotangent * upv * sigma * (1.0 + gate * (1.0 - sigma))
                dcat[rs, 256 * c : 256 * c + 128] = delta_gate.astype(BF16)
                dcat[rs, 256 * c + 128 : 256 * c + 256] = delta_up.astype(BF16)

        def chunk(by):
            return (z + nz + by) % nz

        def partials(offsets, rs):
            rhs = jnp.concatenate(
                [jnp.concatenate([wq[q, chunk(by)] for q in range(4)], 1) for by in offsets], 0
            )
            block = lax.dot_general(
                dcat[rs, :], rhs, (((1,), (1,)), ((), ())), preferred_element_type=F32
            )
            for i, by in enumerate(offsets):
                pc[by % nz, rs] = block[:, 128 * i : 128 * i + 128]

        ways = (1, -1)

        def length(k, w):
            return 8 if (k + w) % 2 == 0 else 7

        def gathered(value, n, k, w):
            first = 0 if n > 0 and DOWN[n - 1] <= length(k, w) else 1
            count = 2 if n - 1 in between(DOWN) else 1
            if first < count:
                part = ring_r.at[w, n - 1, k, pl.ds(first, count - first)]
                arrived(part, rs_recv.at[k, w, n - 1])
                for kind in range(first, count):
                    value = value + ring_r[w, n - 1, k, kind].astype(F32)
            return value

        def reduce_send(value, n, k, w, kind, hops):
            ring_s[w, n, k, kind] = value.astype(BF16)
            copy_to(
                ring_s.at[w, n, k, kind], ring_r.at[w, n, k, kind],
                rs_send, rs_recv.at[k, w, n], along(ways[w] * hops),
            )

        def reduce_stop(n, pieces=range(SUB)):
            for k in pieces:
                for w in range(2):
                    if DOWN[n] <= length(k, w):
                        value = gathered(pc[ways[w] * DOWN[n] % nz, at(k)], n, k, w)
                        reduce_send(value, n, k, w, 0, DOWN[n] - DOWN[n + 1])
                    if n in between(DOWN):
                        reduce_send(pc[ways[w] * (DOWN[n] - 1) % nz, at(k)], n, k, w, 1, 1)

        for h in range(2):
            rs = pl.ds(h * (rows // 2), rows // 2)
            deltas(rs)
            partials((8, 7, -7, 6), rs)
            reduce_stop(0, range(h * (SUB // 2), (h + 1) * (SUB // 2)))
        every = pl.ds(0, rows)
        partials((-6, 5, -5, 4), every)
        partials((-4, 3, -3, 2), every)
        partials((-2, 1, -1, 0), every)
        copy_to(dcat, dcat, share_send.at[0], share_recv.at[0], partner)
        copy_to(gg_h, grads.at[2], give_send.at[0], grads_recv, partner)
        copy_to(gu_h, grads.at[3], give_send.at[1], grads_recv, partner)
        copy_to(wq, wq, share_send.at[1], share_recv.at[1], partner)
        for n in range(1, len(DOWN) - 1):
            reduce_stop(n)

        def spread(n, k, w, origin):
            part = gi.at[origin, at(k)]
            if n + 1 < len(UP) and UP[n + 1] <= length(k, w):
                copy_to(part, part, out_send, out_recv.at[k, w, n], along(ways[w] * (UP[n + 1] - UP[n])))
            if n in between(UP):
                j = between(UP).index(n)
                copy_to(part, part, out_send, out_side_recv.at[w, j], along(ways[w]))

        def to_partner(part):
            copy_to(part, part, d2_send, d2_recv, partner)

        for k in range(SUB):
            value = pc[0, at(k)]
            for w in range(2):
                value = gathered(value, len(DOWN) - 1, k, w)
            gi[z, at(k)] = value.astype(BF16)
            for w in range(2):
                spread(0, k, w, z)
        to_partner(gi.at[z])

        for n in range(len(UP) - 1):
            for k in range(SUB):
                for w in range(2):
                    if UP[n + 1] <= length(k, w):
                        origin = chunk(-ways[w] * UP[n + 1])
                        arrived(gi.at[origin, at(k)], out_recv.at[k, w, n])
                        spread(n + 1, k, w, origin)
                        to_partner(gi.at[origin, at(k)])
            if n in between(UP):
                j = between(UP).index(n)
                for w in range(2):
                    origin = chunk(-ways[w] * (UP[n] + 1))
                    arrived(gi.at[origin], out_side_recv.at[w, j])
                    to_partner(gi.at[origin])

        arrived(hid, hid_recv)
        arrived(ngg, new_recv.at[0])
        arrived(ngu, new_recv.at[1])
        pltpu.make_async_copy(gg_h, gg_h, give_send.at[0]).wait()
        pltpu.make_async_copy(gu_h, gu_h, give_send.at[1]).wait()
        arrived(dcat, share_send.at[0])
        arrived(wq, share_send.at[1])
        arrived(wq.at[pl.ds(0, 2), pl.ds(0, 3)], ag_send.at[0])
        arrived(wq.at[:, pl.ds(0, 12)], ag_send.at[1])
        arrived(gi, d2_send)
        arrived(gi.at[pl.ds(0, nz - 1)], rs_send)
        arrived(gi.at[pl.ds(0, nz - 1)], out_send)


def store(hid, gi, ngg, ngu, hid_o, gi_o, ngg_o, ngu_o, hid_sem, gi_sem, ngg_sem, ngu_sem):
    for o in range(gi.shape[0]):
        pltpu.make_async_copy(gi.at[o], gi_o.at[:, pl.ds(o * 128, 128)], gi_sem).start()
    small = [
        pltpu.make_async_copy(hid, hid_o, hid_sem),
        pltpu.make_async_copy(ngg, ngg_o, ngg_sem),
        pltpu.make_async_copy(ngu, ngu_o, ngu_sem),
    ]
    for copy in small:
        copy.start()
    for copy in small:
        copy.wait()
    pltpu.make_async_copy(gi, gi, gi_sem).wait()


def per_device(nz, x_later, x_earlier, cot_hidden, w_gate, w_up, grad_gate, grad_up):
    rows, width = x_later.shape
    dma = pltpu.SemaphoreType.DMA
    vmem = pltpu.VMEM
    hid, gi, ngg, ngu = pl.pallas_call(
        functools.partial(kernel, nz),
        out_shape=(
            vmem((rows, 128), BF16),
            vmem((nz, rows, 128), BF16),
            vmem((128, 128), F32),
            vmem((128, 128), F32),
        ),
        in_specs=[pl.BlockSpec(memory_space=pl.ANY)] * 7,
        out_specs=(pl.BlockSpec(memory_space=vmem),) * 4,
        scratch_shapes=[
            vmem((rows, width), BF16),
            vmem((rows, width), BF16),
            vmem((2, rows, 128), BF16),
            vmem((2, 128, 128), BF16),
            vmem((4, 128, 128), F32),
            vmem((2, 128, 128), F32),
            vmem((4, 16, 128, 128), BF16),
            vmem((rows, 512), BF16),
            vmem((16, 512, 128), BF16),
            vmem((15, 512, 128), BF16),
            vmem((rows, 128), BF16),
            vmem((nz, rows, 128), F32),
            vmem((2, len(DOWN) - 1, SUB, 2, rows // SUB, 128), BF16),
            vmem((2, len(DOWN) - 1, SUB, 2, rows // SUB, 128), BF16),
            dma((6,)),
            dma((2,)),
            dma((2,)),
            dma((2,)),
            dma((2, 3)),
            dma,
            dma((2,)),
            dma((2,)),
            dma,
            dma,
            dma,
            dma,
            dma,
            dma,
            dma((2,)),
            dma,
            dma((SUB, 2, len(DOWN) - 1)),
            dma,
            dma((SUB, 2, len(UP) - 1)),
            dma((2, max(1, len(between(UP))))),
            dma,
            dma,
        ],
        compiler_params=pltpu.CompilerParams(
            collective_id=0, has_side_effects=True, vmem_limit_bytes=48 * 1024 * 1024
        ),
        name="step",
    )(
        *(
            pltpu.with_memory_space_constraint(operand, pltpu.HBM)
            for operand in (
                x_later,
                x_earlier,
                cot_hidden,
                w_gate,
                w_up,
                grad_gate,
                grad_up,
            )
        )
    )
    any_spec = pl.BlockSpec(memory_space=pl.ANY)
    return pl.pallas_call(
        store,
        out_shape=(
            jax.ShapeDtypeStruct((rows, 128), BF16),
            jax.ShapeDtypeStruct((rows, width), BF16),
            jax.ShapeDtypeStruct((128, 128), F32),
            jax.ShapeDtypeStruct((128, 128), F32),
        ),
        in_specs=[pl.BlockSpec(memory_space=vmem)] * 4,
        out_specs=(any_spec,) * 4,
        scratch_shapes=[dma, dma, dma, dma],
        name="store",
    )(*(pltpu.with_memory_space_constraint(r, vmem) for r in (hid, gi, ngg, ngu)))


def solution(mesh):
    placed = (
        P("fs", None),
        P("fs", None),
        P("fs", "tp"),
        P("fs", "tp"),
        P("fs", "tp"),
        P("fs", "tp"),
        P("fs", "tp"),
    )
    return jax.shard_map(
        functools.partial(per_device, mesh.shape["tp"] // 2),
        mesh=mesh,
        in_specs=placed,
        out_specs=(P("fs", "tp"), P("fs", None), P("fs", "tp"), P("fs", "tp")),
        check_vma=False,
    )
```

time: 58 us -> 57.1 us (0.984)
  Pallas kernels: 57.2 us -> 56.3 us
    pallas_call x1, Pallas kernels: 56 us -> 55 us  [per_device(): pl.pallas_call(functools.partial(kernel, nz), out_shape=(vmem((rows, 128)...]
where the time goes in v4:
time: 57.1 us; the launch traced here: 56.9 us
  Pallas kernels  56.3 us (99%)
  between operations  0.64 us (1%)
    pallas_call x1, Pallas kernels, per_device(): pl.pallas_call(functools.partial(kernel, nz), out_shape=(vmem((rows, 128)...  55 us
    pallas_call x1, Pallas kernels, per_device(): pl.pallas_call(store, out_shape=(jax.ShapeDtypeStruct((rows, 128), BF16),...  1.24 us

profile of v4, /device:TPU:1, one launch (start us, length us, event | category | flops | bytes accessed | tf_op | source)
XLA Modules:
  0.0 56.9 jit_solution(17538567511947004026)
XLA Ops:
  0.6 55.0 %step.1 = (bf16[384,128]{1,0:T(8,128)(2,1)S(1)}, bf16[16,384,128]{2,1,0:T(8,128)(2,1)S(1)}, f32[128,128]{1,0:T(8,128)S(1)}, f32[128,128]{1,0:T(8,128)S(1)}) custom-call(bf16[384,2048]{1,0:T(8,128)(2,1)} %xl_h.1, bf16[384,2048]{1,0:T(8,128)(2,1)} %xe_h.1, bf16[384,128]{1,0:T(8,128)(2,1)} %cot_h.1, bf16[128,128]{1,0:T(8,128)(2,1)} %wg_h.1, ...), custom_call_target="tpu_custom_call" | custom-call | tf_op jit(solution)/shard_map/step/pallas_call | solution.py:327
  55.7 1.2 %store.1 = (bf16[384,128]{1,0:T(8,128)(2,1)}, bf16[384,2048]{1,0:T(8,128)(2,1)}, f32[128,128]{1,0:T(8,128)}, f32[128,128]{1,0:T(8,128)}) custom-call(bf16[384,128]{1,0:T(8,128)(2,1)S(1)} %get-tuple-element.8.hid, bf16[16,384,128]{2,1,0:T(8,128)(2,1)S(1)} %get-tuple-element.9.gi, f32[128,128]{1,0:T(8,128)S(1)} %get-tuple-element.10.ngg, ...), custom_call_target="tpu_custom_call" | custom-call | tf_op jit(solution)/shard_map/store/pallas_call | solution.py:394

commit v5 on v4

--- a/solution.py
+++ b/solution.py
@@ -8,7 +8,7 @@
 from jax.sharding import PartitionSpec as P
 
 MESH = pl.DeviceIdType.MESH
-SUB = 6
+SUB = 8
 DOWN = (8, 6, 4, 2, 0)
 UP = (0, 2, 4, 6, 8)
 F32 = jnp.float32
@@ -256,10 +256,13 @@
         for n in range(1, len(DOWN) - 1):
             reduce_stop(n)
 
+        def out_sem(k, w, n):
+            return rs_recv.at[k, 1 - w, 2 - n] if n < 3 else out_recv.at[k]
+
         def spread(n, k, w, origin):
             part = gi.at[origin, at(k)]
             if n + 1 < len(UP) and UP[n + 1] <= length(k, w):
-                copy_to(part, part, out_send, out_recv.at[k, w, n], along(ways[w] * (UP[n + 1] - UP[n])))
+                copy_to(part, part, out_send, out_sem(k, w, n), along(ways[w] * (UP[n + 1] - UP[n])))
             if n in between(UP):
                 j = between(UP).index(n)
                 copy_to(part, part, out_send, out_side_recv.at[w, j], along(ways[w]))
@@ -281,7 +284,7 @@
                 for w in range(2):
                     if UP[n + 1] <= length(k, w):
                         origin = chunk(-ways[w] * UP[n + 1])
-                        arrived(gi.at[origin, at(k)], out_recv.at[k, w, n])
+                        arrived(gi.at[origin, at(k)], out_sem(k, w, n))
                         spread(n + 1, k, w, origin)
                         to_partner(gi.at[origin, at(k)])
             if n in between(UP):
@@ -367,7 +370,7 @@
             dma,
             dma((SUB, 2, len(DOWN) - 1)),
             dma,
-            dma((SUB, 2, len(UP) - 1)),
+            dma((SUB,)),
             dma((2, max(1, len(between(UP))))),
             dma,
             dma,

time: 57.1 us -> 56.5 us (0.989)
  Pallas kernels: 56.3 us -> 55.7 us
    pallas_call x1, Pallas kernels: 55 us -> 54.4 us  [per_device(): pl.pallas_call(functools.partial(kernel, nz), out_shape=(vmem((rows, 128)...]
where the time goes in v5:
time: 56.5 us; the launch traced here: 56.3 us
  Pallas kernels  55.7 us (99%)
  between operations  0.64 us (1%)
    pallas_call x1, Pallas kernels, per_device(): pl.pallas_call(functools.partial(kernel, nz), out_shape=(vmem((rows, 128)...  54.4 us
    pallas_call x1, Pallas kernels, per_device(): pl.pallas_call(store, out_shape=(jax.ShapeDtypeStruct((rows, 128), BF16),...  1.24 us

profile of v5, /device:TPU:1, one launch (start us, length us, event | category | flops | bytes accessed | tf_op | source)
XLA Modules:
  0.0 56.3 jit_solution(5540826795489716558)
XLA Ops:
  0.6 54.4 %step.1 = (bf16[384,128]{1,0:T(8,128)(2,1)S(1)}, bf16[16,384,128]{2,1,0:T(8,128)(2,1)S(1)}, f32[128,128]{1,0:T(8,128)S(1)}, f32[128,128]{1,0:T(8,128)S(1)}) custom-call(bf16[384,2048]{1,0:T(8,128)(2,1)} %xl_h.1, bf16[384,2048]{1,0:T(8,128)(2,1)} %xe_h.1, bf16[384,128]{1,0:T(8,128)(2,1)} %cot_h.1, bf16[128,128]{1,0:T(8,128)(2,1)} %wg_h.1, ...), custom_call_target="tpu_custom_call" | custom-call | tf_op jit(solution)/shard_map/step/pallas_call | solution.py:330
  55.1 1.2 %store.1 = (bf16[384,128]{1,0:T(8,128)(2,1)}, bf16[384,2048]{1,0:T(8,128)(2,1)}, f32[128,128]{1,0:T(8,128)}, f32[128,128]{1,0:T(8,128)}) custom-call(bf16[384,128]{1,0:T(8,128)(2,1)S(1)} %get-tuple-element.8.hid, bf16[16,384,128]{2,1,0:T(8,128)(2,1)S(1)} %get-tuple-element.9.gi, f32[128,128]{1,0:T(8,128)S(1)} %get-tuple-element.10.ngg, ...), custom_call_target="tpu_custom_call" | custom-call | tf_op jit(solution)/shard_map/store/pallas_call | solution.py:397

commit v6 on v5

--- a/solution.py
+++ b/solution.py
@@ -286,7 +286,10 @@
                         origin = chunk(-ways[w] * UP[n + 1])
                         arrived(gi.at[origin, at(k)], out_sem(k, w, n))
                         spread(n + 1, k, w, origin)
-                        to_partner(gi.at[origin, at(k)])
+                        if UP[n + 1] == 8:
+                            to_partner(gi.at[origin, at(k)])
+                        elif k == SUB - 1:
+                            to_partner(gi.at[origin])
             if n in between(UP):
                 j = between(UP).index(n)
                 for w in range(2):

time: 56.5 us -> 56.5 us (level)
  no operation moved by 1% of the time
where the time goes in v6:
time: 56.5 us; the launch traced here: 56.3 us
  Pallas kernels  55.7 us (99%)
  between operations  0.64 us (1%)
    pallas_call x1, Pallas kernels, per_device(): pl.pallas_call(functools.partial(kernel, nz), out_shape=(vmem((rows, 128)...  54.4 us
    pallas_call x1, Pallas kernels, per_device(): pl.pallas_call(store, out_shape=(jax.ShapeDtypeStruct((rows, 128), BF16),...  1.24 us

profile of v6, /device:TPU:1, one launch (start us, length us, event | category | flops | bytes accessed | tf_op | source)
XLA Modules:
  0.0 56.3 jit_solution(1042993136173749158)
XLA Ops:
  0.6 54.4 %step.1 = (bf16[384,128]{1,0:T(8,128)(2,1)S(1)}, bf16[16,384,128]{2,1,0:T(8,128)(2,1)S(1)}, f32[128,128]{1,0:T(8,128)S(1)}, f32[128,128]{1,0:T(8,128)S(1)}) custom-call(bf16[384,2048]{1,0:T(8,128)(2,1)} %xl_h.1, bf16[384,2048]{1,0:T(8,128)(2,1)} %xe_h.1, bf16[384,128]{1,0:T(8,128)(2,1)} %cot_h.1, bf16[128,128]{1,0:T(8,128)(2,1)} %wg_h.1, ...), custom_call_target="tpu_custom_call" | custom-call | tf_op jit(solution)/shard_map/step/pallas_call | solution.py:333
  55.1 1.2 %store.1 = (bf16[384,128]{1,0:T(8,128)(2,1)}, bf16[384,2048]{1,0:T(8,128)(2,1)}, f32[128,128]{1,0:T(8,128)}, f32[128,128]{1,0:T(8,128)}) custom-call(bf16[384,128]{1,0:T(8,128)(2,1)S(1)} %get-tuple-element.8.hid, bf16[16,384,128]{2,1,0:T(8,128)(2,1)S(1)} %get-tuple-element.9.gi, f32[128,128]{1,0:T(8,128)S(1)} %get-tuple-element.10.ngg, ...), custom_call_target="tpu_custom_call" | custom-call | tf_op jit(solution)/shard_map/store/pallas_call | solution.py:400

commit v7 on v6

--- a/solution.py
+++ b/solution.py
@@ -77,9 +77,9 @@
         load_xl = pltpu.make_async_copy(xl_h, xl, in_sem.at[5])
         load_gg = pltpu.make_async_copy(gg_h, grads.at[0], in_sem.at[1])
         load_gu = pltpu.make_async_copy(gu_h, grads.at[1], in_sem.at[2])
-        greet(partner)
         load_wg.start()
         load_wu.start()
+        greet(partner)
         pl.semaphore_wait(barrier, 4)
         load_wg.wait()
         load_wu.wait()
@@ -140,13 +140,15 @@
         load_wg = pltpu.make_async_copy(wg_h, wq.at[2, f], in_sem.at[3])
         load_wu = pltpu.make_async_copy(wu_h, wq.at[3, f], in_sem.at[4])
         load_cot = pltpu.make_async_copy(cot_h, cot.at[1], in_sem.at[5])
+        for load in (load_wg, load_wu):
+            load.start()
         greet(partner)
         for by in (1, 2, 3):
             greet(beside(0, by, 0))
             greet(beside(1, by, 1))
         for by in (-2, -1, 1, 2):
             greet(along(by))
-        for load in (load_wg, load_wu, load_xe, load_cot):
+        for load in (load_xe, load_cot):
             load.start()
         pl.semaphore_wait(barrier, 8)
 

time: 56.5 us -> 56.5 us (level)
  no operation moved by 1% of the time
where the time goes in v7:
time: 56.5 us; the launch traced here: 56.3 us
  Pallas kernels  55.7 us (99%)
  between operations  0.64 us (1%)
    pallas_call x1, Pallas kernels, per_device(): pl.pallas_call(functools.partial(kernel, nz), out_shape=(vmem((rows, 128)...  54.4 us
    pallas_call x1, Pallas kernels, per_device(): pl.pallas_call(store, out_shape=(jax.ShapeDtypeStruct((rows, 128), BF16),...  1.24 us

profile of v7, /device:TPU:1, one launch (start us, length us, event | category | flops | bytes accessed | tf_op | source)
XLA Modules:
  0.0 56.3 jit_solution(515717638770453879)
XLA Ops:
  0.6 54.4 %step.1 = (bf16[384,128]{1,0:T(8,128)(2,1)S(1)}, bf16[16,384,128]{2,1,0:T(8,128)(2,1)S(1)}, f32[128,128]{1,0:T(8,128)S(1)}, f32[128,128]{1,0:T(8,128)S(1)}) custom-call(bf16[384,2048]{1,0:T(8,128)(2,1)} %xl_h.1, bf16[384,2048]{1,0:T(8,128)(2,1)} %xe_h.1, bf16[384,128]{1,0:T(8,128)(2,1)} %cot_h.1, bf16[128,128]{1,0:T(8,128)(2,1)} %wg_h.1, ...), custom_call_target="tpu_custom_call" | custom-call | tf_op jit(solution)/shard_map/step/pallas_call | solution.py:335
  55.1 1.2 %store.1 = (bf16[384,128]{1,0:T(8,128)(2,1)}, bf16[384,2048]{1,0:T(8,128)(2,1)}, f32[128,128]{1,0:T(8,128)}, f32[128,128]{1,0:T(8,128)}) custom-call(bf16[384,128]{1,0:T(8,128)(2,1)S(1)} %get-tuple-element.8.hid, bf16[16,384,128]{2,1,0:T(8,128)(2,1)S(1)} %get-tuple-element.9.gi, f32[128,128]{1,0:T(8,128)S(1)} %get-tuple-element.10.ngg, ...), custom_call_target="tpu_custom_call" | custom-call | tf_op jit(solution)/shard_map/store/pallas_call | solution.py:402
